TPU v7x, 256 devices: a whole 4x4x8 slice. The times are simulated.
256 devices in a mesh: sp: 32 (over z, x), tp: 8 (over y, core).
Axes of the slice: x: 4, y: 4, z: 8, core: 2. Of those that a mesh axis runs over, the one named last changes fastest.
Arguments:
- out_grad: bfloat16 [4096, 2048], P('sp', 'tp'), may hold values from -6 to 6
- moe_input: bfloat16 [4096, 2048], P('sp', 'tp'), may hold values from -6 to 6
- route_weight: float32 [4096, 2], P('sp'), may hold values from 0.2 to 1
- route_ids: int32 [4096, 2], P('sp'), may hold values from 0 to 31, all different within a row; in each aligned block of 128 rows (0 to 127, 128 to 255, ...) at most 16 rows name the same one
- gate_proj: bfloat16 [32, 2048, 2816], P('sp', None, 'tp'), may hold values from -0.125 to 0.125
- up_proj: bfloat16 [32, 2048, 2816], P('sp', None, 'tp'), may hold values from -0.125 to 0.125
- down_proj: bfloat16 [32, 2816, 2048], P('sp', 'tp'), may hold values from -0.109375 to 0.109375
- out_proj: bfloat16 [2048, 2048], P(None, 'tp'), may hold values from -0.125 to 0.125
- conv_out: bfloat16 [4096, 2048], P('sp', 'tp'), may hold values from -6 to 6
- gate_b: bfloat16 [4096, 2048], P('sp', 'tp'), may hold values from -6 to 6
- gate_c: bfloat16 [4096, 2048], P('sp', 'tp'), may hold values from -6 to 6
- value_v: bfloat16 [4096, 2048], P('sp', 'tp'), may hold values from -6 to 6
- conv_taps: float32 [3, 2048], P(None, 'tp'), may hold values from -3 to 3
Outputs:
- grad_gate: bfloat16 [32, 2048, 2816], P('sp', None, 'tp')
- grad_up: bfloat16 [32, 2048, 2816], P('sp', None, 'tp')
- grad_down: bfloat16 [32, 2816, 2048], P('sp', 'tp')
- grad_out: float32 [2048, 2048], P('sp', 'tp')
- grad_b: bfloat16 [4096, 2048], P('sp', 'tp')
- grad_c: bfloat16 [4096, 2048], P('sp', 'tp')
- grad_v: bfloat16 [4096, 2048], P('sp', 'tp')
Inputs may be any that keep to these rules, and one draw needn't show every extreme that they name: `route_ids`: each row names two different experts; within the 128 rows of one index of sp no expert is named by more than 16 rows, a bound that some block reaches.
All inputs are finite; a program needn't handle non-finite values.
Results may differ from a plain program's by a relative error of at most 0.019.
Values may be sent and summed in bfloat16 or wider, within the bound.
A program may use at most 64 MiB of HBM per device.

v0:
```python
import jax
import jax.numpy as jnp
from jax import lax
from jax.sharding import Mesh
from jax.sharding import PartitionSpec as P

SP = ("sp_0", "sp_1")


def sent_together(arrays, axis, split_dim, concat_dim, along):
    ends, at = ([], 0)
    for a in arrays[:-1]:
        at += a.shape[along]
        ends.append(at)
    both = jnp.concatenate(arrays, axis=along)
    return tuple(
        jnp.split(
            lax.all_to_all(both, axis, split_axis=split_dim, concat_axis=concat_dim, tiled=True),
            ends,
            axis=along,
        )
    )


def in_one_piece(arrays, axis, dim, along):
    ends, at = ([], 0)
    for a in arrays[:-1]:
        at += a.shape[along]
        ends.append(at)
    both = jnp.concatenate(arrays, axis=along)
    return tuple(jnp.split(lax.all_gather(both, axis, axis=dim, tiled=True), ends, axis=along))


def cut_along(x, dim, peers):
    before, after = (x.shape[:dim], x.shape[dim + 1 :])
    return jnp.moveaxis(x.reshape(*before, peers, -1, *after), dim, 0)


def summed_on_arrival(x, axis, dim):
    blocks = cut_along(x, dim, lax.axis_size(axis))
    arrived = lax.all_to_all(blocks, axis, split_axis=0, concat_axis=0, tiled=True)
    return arrived.astype(jnp.float32).sum(axis=0)


def sent_to_all(x, axis):
    copies = jnp.broadcast_to(x, (lax.axis_size(axis), *x.shape))
    return lax.all_to_all(copies, axis, split_axis=0, concat_axis=0, tiled=True)


def laid_out(blocks, dim):
    blocks = jnp.moveaxis(blocks, 0, dim)
    shape = blocks.shape
    return blocks.reshape(*shape[:dim], shape[dim] * shape[dim + 1], *shape[dim + 2 :])


def collect(x, axis, dim):
    blocks = sent_to_all(x, axis)
    return laid_out(blocks, dim)


def with_halo(block, sides, width):
    for axis, dim in sides:
        count = lax.axis_size(axis)
        forward = [(i, i + 1) for i in range(count - 1)]
        backward = [(target, source) for source, target in forward]
        low = lax.ppermute(
            lax.slice_in_dim(block, block.shape[dim] - width, None, axis=dim), axis, forward
        )
        high = lax.ppermute(lax.slice_in_dim(block, 0, width, axis=dim), axis, backward)
        block = jnp.concatenate([low, block, high], axis=dim)
    return block


def cut_rows(length, count):
    unit = 8 if length >= 8 * count else 1
    return [length // unit * k // count * unit for k in range(1, count)]


def own_block(blocks, axes, sequence):
    inside = blocks.shape[1:]
    blocks = blocks.reshape(*(lax.axis_size(a) for a in axes), *inside)
    blocks = jnp.moveaxis(blocks, sequence, range(len(axes))).reshape(-1, *inside)
    for k in sequence:
        blocks = lax.psum_scatter(blocks, axes[k], scatter_dimension=0, tiled=True)
    return blocks[0]


def sum_at_once(x, axes, dim):
    blocks = cut_along(x, dim, lax.axis_size(axes))
    split_at = max(range(1, max(2, blocks.ndim - 1)), key=lambda d: blocks.shape[d])
    count, finished = (len(axes), [])
    for initial, section in enumerate(
        jnp.split(blocks, cut_rows(blocks.shape[split_at], count), axis=split_at)
    ):
        if section.size:
            sequence = [(initial + k) % count for k in range(count)]
            finished.append(own_block(section, axes, sequence))
    return jnp.concatenate(finished, axis=split_at - 1)


def place_rows(rows, index, total):
    return jnp.zeros((total, rows.shape[1]), rows.dtype).at[index].set(rows)


def local(
    out_grad,
    moe_input,
    route_weight,
    route_ids,
    gate_proj,
    up_proj,
    down_proj,
    out_proj,
    conv_out,
    gate_b,
    gate_c,
    value_v,
    conv_taps,
):
    tok_rows = out_grad.shape[0]
    local_cols = out_grad.shape[1]
    n_experts = lax.axis_size(SP)
    capacity = 4 * tok_rows // n_experts
    flat = route_ids.reshape(2 * tok_rows)
    onehot = (flat[:, None] == jnp.arange(n_experts, dtype=jnp.int32)[None, :]).astype(jnp.int32)
    before = jnp.cumsum(onehot, axis=0) - onehot
    slot = jnp.sum(before * onehot, axis=1)
    dest = flat * capacity + slot
    total = n_experts * capacity
    rows_x = jnp.broadcast_to(moe_input[:, None, :], (tok_rows, 2, local_cols)).reshape(
        2 * tok_rows, local_cols
    )
    rows_dy = (
        (route_weight[:, :, None] * out_grad.astype(jnp.float32)[:, None, :])
        .astype(jnp.bfloat16)
        .reshape(2 * tok_rows, local_cols)
    )
    send_x = place_rows(rows_x, dest, total).reshape(n_experts, capacity, local_cols)
    send_dy = place_rows(rows_dy, dest, total).reshape(n_experts, capacity, local_cols)
    part_x, part_dy = sent_together((send_x, send_dy), SP, 0, 0, 1)
    recv_x, recv_dy = in_one_piece((part_x, part_dy), "tp", 2, 0)
    width = recv_x.shape[2]
    xin = recv_x.reshape(total, width)
    dyin = recv_dy.reshape(total, width)
    w_gate = gate_proj[0]
    w_up = up_proj[0]
    w_down = down_proj[0]
    gate = jnp.dot(xin, w_gate, preferred_element_type=jnp.float32)
    upval = jnp.dot(xin, w_up, preferred_element_type=jnp.float32)
    sig = jax.nn.sigmoid(gate)
    act = gate * sig
    hidden = (act * upval).astype(jnp.bfloat16)
    grad_down = jnp.dot(hidden.T, dyin, preferred_element_type=jnp.float32).astype(jnp.bfloat16)
    dhid = jnp.dot(dyin, w_down.T, preferred_element_type=jnp.float32)
    dgate = (dhid * upval * (sig * (1.0 + gate * (1.0 - sig)))).astype(jnp.bfloat16)
    dup = (dhid * act).astype(jnp.bfloat16)
    grad_gate = jnp.dot(xin.T, dgate, preferred_element_type=jnp.float32).astype(jnp.bfloat16)
    grad_up = jnp.dot(xin.T, dup, preferred_element_type=jnp.float32).astype(jnp.bfloat16)
    partial_value = jnp.dot(dgate, w_gate.T, preferred_element_type=jnp.float32) + jnp.dot(
        dup, w_up.T, preferred_element_type=jnp.float32
    )
    partial_value = lax.optimization_barrier(partial_value.astype(jnp.bfloat16)).astype(jnp.float32)
    summed = summed_on_arrival(partial_value.astype(jnp.bfloat16), "tp", 1).astype(jnp.bfloat16)
    returned = lax.all_to_all(
        summed.reshape(n_experts, capacity, local_cols), SP, split_axis=0, concat_axis=0, tiled=True
    )
    picked = returned.reshape(total, local_cols)[dest]
    moe_grad = jnp.sum(picked.reshape(tok_rows, 2, local_cols).astype(jnp.float32), axis=1)
    grad_h = (out_grad.astype(jnp.float32) + moe_grad).astype(jnp.bfloat16)
    full_h = collect(grad_h, "tp", 1)
    grad_z = jnp.dot(full_h, out_proj, preferred_element_type=jnp.float32)
    dconv = (grad_z * gate_b.astype(jnp.float32)).astype(jnp.bfloat16)
    grad_b = (grad_z * conv_out.astype(jnp.float32)).astype(jnp.bfloat16)
    padded = with_halo(dconv, ((SP, 0),), 1).astype(jnp.float32)
    grad_u = conv_taps[0] * padded[2:] + conv_taps[1] * padded[1:-1] + conv_taps[2] * padded[:-2]
    grad_c = (grad_u * value_v.astype(jnp.float32)).astype(jnp.bfloat16)
    grad_v = (grad_u * gate_c.astype(jnp.float32)).astype(jnp.bfloat16)
    mixed = (gate_b.astype(jnp.float32) * conv_out.astype(jnp.float32)).astype(jnp.bfloat16)
    grad_out = sum_at_once(
        lax.dot_general(
            full_h, mixed, (((0,), (0,)), ((), ())), preferred_element_type=jnp.float32
        ).astype(jnp.bfloat16),
        SP,
        0,
    ).astype(jnp.float32)
    return (grad_gate[None], grad_up[None], grad_down[None], grad_out, grad_b, grad_c, grad_v)


def solution(mesh):
    split = Mesh(mesh.devices.reshape(8, 4, mesh.shape["tp"]), ("sp_0", "sp_1", "tp"))
    return jax.shard_map(
        local,
        mesh=split,
        in_specs=(
            P(SP, "tp"),
            P(SP, "tp"),
            P(SP, None),
            P(SP, None),
            P(SP, None, "tp"),
            P(SP, None, "tp"),
            P(SP, "tp", None),
            P(None, "tp"),
            P(SP, "tp"),
            P(SP, "tp"),
            P(SP, "tp"),
            P(SP, "tp"),
            P(None, "tp"),
        ),
        out_specs=(
            P(SP, None, "tp"),
            P(SP, None, "tp"),
            P(SP, "tp", None),
            P(SP, "tp"),
            P(SP, "tp"),
            P(SP, "tp"),
            P(SP, "tp"),
        ),
        check_vma=False,
    )
```

profile of v0, /device:TPU:1, one launch (start us, length us, event | category | flops | bytes accessed | tf_op | source)
XLA Modules:
  0.0 286.4 jit_solution(10276640265390173089)
XLA Ops:
  13.3 1.5 scatter_custom_fusion
  14.8 1.6 scatter_custom_fusion.1
  16.5 27.9 %all_to_all.20 = bf16[32,32,256]{2,1,0:T(8,128)(2,1)S(1)} all-to-all(bf16[32,32,256]{2,1,0:T(8,128)(2,1)S(1)} %pad_maximum_fusion), channel_id=1, replica_groups=mesh['sp_0'=8,'sp_1'=4,'tp'=8] {'sp_0','sp_1'}, dimensions={0} | all-to-all | bytes 1048576 | tf_op jit(solution)/shard_map/all_to_all | solution.py:18
  45.4 36.7 %all-gather.2.cloned.1.call-done = bf16[64,16,2048]{2,1,0:T(8,128)(2,1)} async-done(((bf16[64,16,256]{2,1,0:T(8,128)(2,1)}), bf16[64,16,2048]{2,1,0:T(8,128)(2,1)}) %all-gather.2.cloned.1.call-update) | async-done | bytes 4194320 | tf_op jit(solution)/shard_map/all_gather | solution.py:31
  82.1 2.7 fusion.31
  86.2 1.1 copy-done.4
  88.9 1.2 multiply_convert_fusion.1
  90.1 1.3 fusion.3
  91.4 1.4 add_convert_fusion
  92.9 30.2 %all_to_all.21 = bf16[8,512,256]{2,1,0:T(8,128)(2,1)S(1)} all-to-all(bf16[8,512,256]{2,1,0:T(8,128)(2,1)S(1)} %bitcast.81), channel_id=1, replica_groups=mesh['sp_0'=8,'sp_1'=4,'tp'=8] {'tp'}, dimensions={0} | all-to-all | bytes 4194304 | tf_op jit(solution)/shard_map/all_to_all | solution.py:41
  124.2 9.7 %all-to-all-start.2 = ((bf16[32,16,256]{2,1,0:T(8,128)(2,1)}), bf16[32,16,256]{2,1,0:T(8,128)(2,1)S(1)}, u32[]{:S(2)}, u32[]{:S(2)}) async-start(bf16[32,16,256]{2,1,0:T(8,128)(2,1)} %bitcast.95), calls=%async_computation.2 | async-start | bytes 524288 | tf_op jit(solution)/shard_map/all_to_all | solution.py:164
  133.9 10.5 %all-to-all-done.2 = bf16[32,16,256]{2,1,0:T(8,128)(2,1)S(1)} async-done(((bf16[32,16,256]{2,1,0:T(8,128)(2,1)}), bf16[32,16,256]{2,1,0:T(8,128)(2,1)S(1)}, u32[]{:S(2)}, u32[]{:S(2)}) %all-to-all-start.2) | async-done | bytes 262176 | tf_op jit(solution)/shard_map/all_to_all | solution.py:164
  144.5 1.2 gather_fusion
  146.3 14.7 %all_to_all.22 = bf16[8,128,256]{1,2,0:T(8,128)(2,1)S(1)} all-to-all(bf16[8,128,256]{1,2,0:T(8,128)(2,1)S(1)} %broadcast_in_dim.28), channel_id=1, replica_groups=mesh['sp_0'=8,'sp_1'=4,'tp'=8] {'tp'}, dimensions={0} | all-to-all | bytes 1048576 | tf_op jit(solution)/shard_map/all_to_all | solution.py:47
  163.4 3.8 %fusion.1 = bf16[1,2048,352]{1,2,0:T(8,128)(2,1)} fusion(bf16[512,352]{0,1:T(8,128)(2,1)S(1)} %copy-done.7, bf16[512,2048]{1,0:T(8,128)(2,1)} %bitcast.91), kind=kOutput, calls=%fused_computation.9 | convolution fusion | flops 738918400 | bytes 3899392 | tf_op jit(solution)/shard_map/dot_general | solution.py:157
  167.2 2.1 fusion
  170.3 1.3 collective-permute-start.1
  171.6 4.0 %collective-permute-start = (bf16[1,256]{1,0:T(2,128)(2,1)S(1)}, bf16[1,256]{1,0:T(2,128)(2,1)S(1)}, u32[]{:S(2)}, u32[]{:S(2)}) collective-permute-start(bf16[1,256]{1,0:T(2,128)(2,1)S(1)} %get-tuple-element.19), channel_id=1, source_target_pairs={{0,8},{8,16},{16,24},{24,32},{32,40},{40,48},{48,56},{56,64},{64,7... | collective-permute-start | bytes 1544 | tf_op jit(solution)/shard_map/ppermute | solution.py:66
  175.6 14.0 %reduce-scatter.5.cloned.1.call-done = bf16[4,32,256]{2,1,0:T(8,128)(2,1)} async-done(((bf16[32,32,256]{2,1,0:T(8,128)(2,1)}), bf16[4,32,256]{2,1,0:T(8,128)(2,1)}) %reduce-scatter.5.cloned.1.call-update) | async-done | bytes 65552 | tf_op jit(solution)/shard_map/reduce_scatter | solution.py:84
  189.7 3.6 %fusion.2 = bf16[1,2048,352]{1,2,0:T(8,128)(2,1)} fusion(bf16[512,352]{0,1:T(8,128)(2,1)S(1)} %copy-done.9, bf16[512,2048]{1,0:T(8,128)(2,1)} %bitcast.92), kind=kOutput, calls=%fused_computation.10 | convolution fusion | flops 738918400 | bytes 3899392 | tf_op jit(solution)/shard_map/dot_general | solution.py:158
  193.3 24.0 %reduce-scatter.9.cloned.1.call-done = bf16[8,32,256]{2,1,0:T(8,128)(2,1)} async-done(((bf16[32,32,256]{2,1,0:T(8,128)(2,1)}), bf16[8,32,256]{2,1,0:T(8,128)(2,1)}) %reduce-scatter.9.cloned.1.call-update) | async-done | bytes 131088 | tf_op jit(solution)/shard_map/reduce_scatter | solution.py:84
  218.7 23.9 %reduce-scatter.7.cloned.1.call-done = bf16[1,32,256]{2,1,0:T(8,128)(2,1)} async-done(((bf16[4,32,256]{2,1,0:T(8,128)(2,1)}), bf16[1,32,256]{2,1,0:T(8,128)(2,1)}) %reduce-scatter.7.cloned.1.call-update) | async-done | bytes 16400 | tf_op jit(solution)/shard_map/reduce_scatter | solution.py:84
  242.6 35.9 %reduce-scatter.11.cloned.1.call-done = bf16[1,32,256]{2,1,0:T(8,128)(2,1)} async-done(((bf16[8,32,256]{2,1,0:T(8,128)(2,1)}), bf16[1,32,256]{2,1,0:T(8,128)(2,1)}) %reduce-scatter.11.cloned.1.call-update) | async-done | bytes 16400 | tf_op jit(solution)/shard_map/reduce_scatter | solution.py:84
  278.5 1.4 maximum_convert_fusion.1
  (94 shorter events, 16.6 us)
Async XLA Ops:
  7.2 77.7 %copy-start = (bf16[1,2048,352]{1,2,0:T(8,128)(2,1)S(1)}, bf16[1,2048,352]{1,2,0:T(8,128)(2,1)}, u32[]{:S(2)}) copy-start(bf16[1,2048,352]{1,2,0:T(8,128)(2,1)} %param.17) | copy-start | bytes 4325380
  7.2 74.9 %all-gather.2.cloned.1.call-start = ((), (), s32[]{:S(2)}) async-start(), calls=%async_computation.8 | async-start | bytes 4718592 | tf_op jit(solution)/shard_map/all_gather | solution.py:31
  84.8 3.4 %copy-start.2 = (bf16[32,16,2048]{2,1,0:T(8,128)(2,1)}, bf16[32,16,2048]{2,1,0:T(8,128)(2,1)S(1)}, u32[]{:S(2)}) copy-start(bf16[32,16,2048]{2,1,0:T(8,128)(2,1)S(1)} %get-tuple-element.9) | copy-start | bytes 6291460
  84.8 2.4 copy-start.4
  87.3 1.6 copy-start.16
  88.3 1.8 copy-start.19
  124.2 21.9 %copy-start.10 = (bf16[128,256]{1,0:T(8,128)(2,1)S(1)}, bf16[128,256]{1,0:T(8,128)(2,1)}, u32[]{:S(2)}) copy-start(bf16[128,256]{1,0:T(8,128)(2,1)} %param.13) | copy-start | bytes 196612
  124.2 20.3 %all-to-all-start.2 = ((bf16[32,16,256]{2,1,0:T(8,128)(2,1)}), bf16[32,16,256]{2,1,0:T(8,128)(2,1)S(1)}, u32[]{:S(2)}, u32[]{:S(2)}) async-start(bf16[32,16,256]{2,1,0:T(8,128)(2,1)} %bitcast.95), calls=%async_computation.2 | async-start | bytes 524288 | tf_op jit(solution)/shard_map/all_to_all | solution.py:164
  133.8 27.2 %copy-start.11 = (bf16[128,256]{1,0:T(8,128)(2,1)S(1)}, bf16[128,256]{1,0:T(8,128)(2,1)}, u32[]{:S(2)}) copy-start(bf16[128,256]{1,0:T(8,128)(2,1)} %param.21) | copy-start | bytes 196612
  133.9 27.2 %copy-start.12 = (bf16[128,256]{1,0:T(8,128)(2,1)S(1)}, bf16[128,256]{1,0:T(8,128)(2,1)}, u32[]{:S(2)}) copy-start(bf16[128,256]{1,0:T(8,128)(2,1)} %param.22) | copy-start | bytes 196612
  133.9 55.7 %reduce-scatter.5.cloned.1.call-start = ((), (), s32[]{:S(2)}) async-start(), calls=%async_computation.9 | async-start | bytes 589824 | tf_op jit(solution)/shard_map/reduce_scatter | solution.py:84
  161.5 1.9 copy-start.7
  162.4 54.9 %reduce-scatter.9.cloned.1.call-start = ((), (), s32[]{:S(2)}) async-start(), calls=%async_computation.11 | async-start | bytes 655360 | tf_op jit(solution)/shard_map/reduce_scatter | solution.py:84
  163.3 79.2 %reduce-scatter.7.cloned.1.call-start = ((), (), s32[]{:S(2)}) async-start(), calls=%async_computation.10 | async-start | bytes 81920 | tf_op jit(solution)/shard_map/reduce_scatter | solution.py:84
  163.4 3.8 %copy-start.3 = (bf16[32,16,2048]{2,1,0:T(8,128)(2,1)S(1)}, bf16[32,16,2048]{2,1,0:T(8,128)(2,1)}, u32[]{:S(2)}) copy-start(bf16[32,16,2048]{2,1,0:T(8,128)(2,1)} %copy-done.2) | copy-start | bytes 6291460
  163.4 3.8 %copy-start.18 = (f32[512,352]{0,1:T(8,128)S(1)}, f32[512,352]{0,1:T(8,128)}, u32[]{:S(2)}) copy-start(f32[512,352]{0,1:T(8,128)} %copy-done.17) | copy-start | bytes 2162692
  163.4 3.8 %copy-start.20 = (f32[512,352]{0,1:T(8,128)S(1)}, f32[512,352]{0,1:T(8,128)}, u32[]{:S(2)}) copy-start(f32[512,352]{0,1:T(8,128)} %copy-done.19) | copy-start | bytes 2162692
  167.2 2.1 copy-start.5
  167.2 22.5 %copy-start.9 = (bf16[512,352]{0,1:T(8,128)(2,1)S(1)}, bf16[512,352]{0,1:T(8,128)(2,1)}, u32[]{:S(2)}) copy-start(bf16[512,352]{0,1:T(8,128)(2,1)} %copy-done.8) | copy-start | bytes 1081348
  170.3 23.0 %collective-permute-start.1 = (bf16[1,256]{1,0:T(2,128)(2,1)S(1)}, bf16[1,256]{1,0:T(2,128)(2,1)S(1)}, u32[]{:S(2)}, u32[]{:S(2)}) collective-permute-start(bf16[1,256]{1,0:T(2,128)(2,1)S(1)} %get-tuple-element.20), channel_id=1, source_target_pairs={{8,0},{16,8},{24,16},{32,24},{40,32},{48,40},{56,48},{64,56},{72,6... | collective-permute-start | bytes 1544 | tf_op jit(solution)/shard_map/ppermute | solution.py:69
  171.6 21.7 %collective-permute-start = (bf16[1,256]{1,0:T(2,128)(2,1)S(1)}, bf16[1,256]{1,0:T(2,128)(2,1)S(1)}, u32[]{:S(2)}, u32[]{:S(2)}) collective-permute-start(bf16[1,256]{1,0:T(2,128)(2,1)S(1)} %get-tuple-element.19), channel_id=1, source_target_pairs={{0,8},{8,16},{16,24},{24,32},{32,40},{40,48},{48,56},{56,64},{64,7... | collective-permute-start | bytes 1544 | tf_op jit(solution)/shard_map/ppermute | solution.py:66
  189.6 27.7 %copy-start.13 = (bf16[128,256]{1,0:T(8,128)(2,1)S(1)}, bf16[128,256]{1,0:T(8,128)(2,1)}, u32[]{:S(2)}) copy-start(bf16[128,256]{1,0:T(8,128)(2,1)} %param.23) | copy-start | bytes 196612
  189.6 28.4 %copy-start.14 = (bf16[128,256]{1,0:T(8,128)(2,1)S(1)}, bf16[128,256]{1,0:T(8,128)(2,1)}, u32[]{:S(2)}) copy-start(bf16[128,256]{1,0:T(8,128)(2,1)} %param.24) | copy-start | bytes 196612
  189.6 88.8 %reduce-scatter.11.cloned.1.call-start = ((), (), s32[]{:S(2)}) async-start(), calls=%async_computation.12 | async-start | bytes 147456 | tf_op jit(solution)/shard_map/reduce_scatter | solution.py:84
  (5 other events, 6.4 us)
Sparse Core Ops, SparseCore 0:
  45.5 36.5 all-gather.1
  162.5 27.0 reduce-scatter.4
  192.1 25.1 reduce-scatter.8
  219.6 22.8 reduce-scatter.6
  244.9 33.4 reduce-scatter.10
where the time goes:
time: 292 us; the launch traced here: 286 us
  waiting for transfers between devices  145 us (50%)
  blocking collectives  72.9 us (25%)
  matrix products  16.7 us (6%)
  starting transfers between devices  15.1 us (5%)
  local copies, waits for them, and re-layouts  14.3 us (5%)
  between operations  14.2 us (5%)
  other arithmetic  8.14 us (3%)
    reduce_scatter x4, waiting for transfers between devices, own_block(): blocks = lax.psum_scatter(blocks, axes[k], scatter_dimension=0, tiled=True)  97.7 us
    all_gather x1, waiting for transfers between devices, in_one_piece(): lax.all_gather(both, axis, axis=dim, tiled=True)  36.7 us
    all_to_all x1, blocking collectives, summed_on_arrival(): lax.all_to_all(blocks, axis, split_axis=0, concat_axis=0, tiled=True)  30.2 us
    all_to_all x1, blocking collectives, sent_together(): lax.all_to_all(both, axis, split_axis=split_dim, concat_axis=concat_dim,...  27.9 us
    all_to_all x1, blocking collectives, sent_to_all(): return lax.all_to_all(copies, axis, split_axis=0, concat_axis=0, tiled=True)  14.7 us
    all_to_all x1, waiting for transfers between devices, local(): lax.all_to_all(summed.reshape(n_experts, capacity, local_cols), SP, split...  10.5 us
    all_to_all x1, starting transfers between devices, local(): lax.all_to_all(summed.reshape(n_experts, capacity, local_cols), SP, split...  9.67 us
  transfers between devices with their start and end apart: 8, of which 6 were waited for; matrix products, arithmetic and copies ran while one was open for 4% of the time, Pallas kernels for 0%

commit v1 on v0

v1 whole, which is shorter than its diff:
```python
import jax
import jax.numpy as jnp
from jax import lax
from jax.experimental import pallas as pl
from jax.experimental.pallas import tpu as pltpu
from jax.sharding import PartitionSpec as P

MESH = pl.DeviceIdType.MESH
BF = jnp.bfloat16
F32 = jnp.float32
NZ, NX, NY = 8, 4, 4
NSP = NZ * NX
CAP = 16
TOK = 128
CH = 256
D = 2048
FFL = 352
OFF = 384
ROWS = NSP * CAP
CHUNKS = 4
CR = ROWS // CHUNKS


def dot(a, b, ca, cb):
    return lax.dot_general(a, b, (((ca,), (cb,)), ((), ())), preferred_element_type=F32)


def offset_of(k):
    odd = k % 2
    return odd * ((k + 1) // 2) + (1 - odd) * ((NZ - k // 2) % NZ)


def kernel(
    out_grad,
    moe_input,
    route_weight,
    ids_t,
    gate_proj,
    up_proj,
    down_proj,
    out_proj,
    conv_out,
    gate_b,
    gate_c,
    value_v,
    taps,
    g_gate,
    g_up,
    g_down,
    g_out,
    g_b,
    g_c,
    g_v,
    send,
    xd,
    wg,
    wu,
    wd,
    wo,
    place,
    dgu,
    hid_t,
    part,
    sib,
    ssum,
    rl,
    rr,
    fl,
    fr,
    rsum,
    ret,
    hf,
    js,
    dt,
    mx,
    hsend,
    halo,
    og_gate,
    og_up,
    og_down,
    w_sem,
    o_sem,
    a_send,
    a_recv,
    b_send,
    b_recv,
    d_send,
    d_recv,
    e_send,
    e_recv,
    h_send,
    h_recv,
    j_send,
    j_recv,
    k_send,
    k_recv,
    m_send,
    m_recv,
    n_send,
    n_recv,
):
    s = lax.axis_index("sp")
    t = lax.axis_index("tp")
    z, x = s // NX, s % NX
    y, c = t // 2, t % 2
    up, down, far = (y + 1) % NY, (y + NY - 1) % NY, (y + 2) % NY
    t_up, t_down, t_sib = up * 2 + c, down * 2 + c, y * 2 + (1 - c)
    t_far = far * 2 + c

    def remote(src, dst, ssem, rsem, sp, tp):
        return pltpu.make_async_remote_copy(
            src_ref=src,
            dst_ref=dst,
            send_sem=ssem,
            recv_sem=rsem,
            device_id={"sp": sp, "tp": tp},
            device_id_type=MESH,
        )

    def arrived(ref, rsem):
        remote(ref, ref, n_send.at[0], rsem, s, t).wait_recv()

    def left(ref, ssem):
        remote(ref, ref, ssem, n_recv.at[0], s, t).wait_send()

    barrier = pltpu.get_barrier_semaphore()

    def greet(i, carry):
        pl.semaphore_signal(
            barrier, inc=1, device_id={"sp": (s + i) % NSP, "tp": t}, device_id_type=MESH
        )
        return carry

    lax.fori_loop(1, NSP, greet, 0)
    for peer in (t_up, t_down, t_sib):
        pl.semaphore_signal(barrier, inc=1, device_id={"sp": s, "tp": peer}, device_id_type=MESH)
    for j in range(NX):

        @pl.when(jnp.logical_not(jnp.logical_and(z == t, x == j)))
        def _():
            pl.semaphore_signal(
                barrier, inc=1, device_id={"sp": t * NX + j, "tp": z}, device_id_type=MESH
            )

    loads = [
        pltpu.make_async_copy(gate_proj.at[0], wg, w_sem.at[0]),
        pltpu.make_async_copy(up_proj.at[0], wu, w_sem.at[1]),
        pltpu.make_async_copy(down_proj.at[0], wd, w_sem.at[2]),
        pltpu.make_async_copy(out_proj, wo, w_sem.at[3]),
    ]
    for load in loads:
        load.start()

    ids = ids_t[...]
    experts = lax.broadcasted_iota(jnp.int32, (NSP, TOK), 0)
    e0 = jnp.where(experts == ids[0:1, :], 1.0, 0.0).astype(F32)
    e1 = jnp.where(experts == ids[1:2, :], 1.0, 0.0).astype(F32)
    row = lax.broadcasted_iota(jnp.int32, (TOK, TOK), 0)
    col = lax.broadcasted_iota(jnp.int32, (TOK, TOK), 1)
    earlier = jnp.where(row < col, 1.0, 0.0).astype(BF)
    before = dot((e0 + e1).astype(BF), earlier, 1, 0)
    slot0 = jnp.sum(before * e0, axis=0, keepdims=True)
    slot1 = jnp.sum(before * e1, axis=0, keepdims=True)
    idf = ids.astype(F32) * CAP
    at = lax.broadcasted_iota(jnp.int32, (ROWS, TOK), 0).astype(F32)
    p0 = jnp.where(at == idf[0:1, :] + slot0, 1.0, 0.0).astype(BF)
    p1 = jnp.where(at == idf[1:2, :] + slot1, 1.0, 0.0).astype(BF)
    place[...] = p0 + p1
    og = out_grad[...].astype(F32)
    w = route_weight[...]
    dy0 = (w[:, 0:1] * og).astype(BF)
    dy1 = (w[:, 1:2] * og).astype(BF)
    send[0] = dot(p0 + p1, moe_input[...], 1, 0).astype(BF)
    send[1] = (dot(p0, dy0, 1, 0) + dot(p1, dy1, 1, 0)).astype(BF)
    mixed = (gate_b[...].astype(F32) * conv_out[...].astype(F32)).astype(BF)
    own_rows = pl.ds(pl.multiple_of(s * TOK, TOK), TOK)
    mx[own_rows, :] = mixed
    dgu[...] = jnp.zeros_like(dgu)

    def cols(tp, width=CH):
        return pl.ds(pl.multiple_of(tp * width, width), width)

    pl.semaphore_wait(barrier, NSP - 1 + 3 + 4 - jnp.where(z == t, 1, 0))

    def a_copy(i):
        k, dx = i // NX, i % NX
        target = ((z + offset_of(k)) % NZ) * NX + (x + dx) % NX
        src = send.at[:, pl.ds(pl.multiple_of(target * CAP, CAP), CAP), :]
        dst = xd.at[:, pl.ds(pl.multiple_of(k * NX * CAP + x * CAP, CAP), CAP), cols(t)]
        return remote(src, dst, a_send.at[i], a_recv.at[k * NX + x], target, t)

    def a_start(i, carry):
        a_copy(i).start()
        return carry

    lax.fori_loop(1, NSP, a_start, 0)
    here = pl.ds(pl.multiple_of(x * CAP, CAP), CAP)
    xd[:, here, cols(t)] = send[:, pl.ds(pl.multiple_of(s * CAP, CAP), CAP), :]

    x_peers = [(1, (x + 1) % NX, (x + 3) % NX), (3, (x + 3) % NX, (x + 1) % NX), (2, (x + 2) % NX, (x + 2) % NX)]
    for i, (_, to, _from) in enumerate(x_peers):
        remote(
            mx.at[own_rows, :], mx.at[own_rows, :], m_send.at[i], m_recv.at[i], z * NX + to, t
        ).start()

    def a_wait(k, first):
        def body(i, carry):
            xx = (x + i) % NX
            arrived(
                xd.at[:, pl.ds(pl.multiple_of(k * NX * CAP + xx * CAP, CAP), CAP), cols(t)],
                a_recv.at[k * NX + xx],
            )
            return carry

        lax.fori_loop(first, NX, body, 0)

    def gather(piece, ss, rs):
        def one():
            remote(piece(t), piece(t), ss(0), rs(0), s, t_up).start()
            remote(piece(t), piece(t), ss(1), rs(1), s, t_down).start()
            remote(piece(t), piece(t), ss(4), rs(4), s, t_sib).start()

        def two():
            arrived(piece(t_down), rs(0))
            remote(piece(t_down, 0), piece(t_down, 0), ss(2), rs(2), s, t_up).start()
            remote(piece(t_down), piece(t_down), ss(5), rs(5), s, t_sib).start()
            arrived(piece(t_up), rs(1))
            remote(piece(t_up, 1), piece(t_up, 1), ss(3), rs(3), s, t_down).start()
            remote(piece(t_up), piece(t_up), ss(6), rs(6), s, t_sib).start()

        def three():
            arrived(piece(t_far, 0), rs(2))
            remote(piece(t_far, 0), piece(t_far, 0), ss(7), rs(7), s, t_sib).start()
            arrived(piece(t_far, 1), rs(3))
            remote(piece(t_far, 1), piece(t_far, 1), ss(8), rs(8), s, t_sib).start()

        def four():
            arrived(piece(t_sib), rs(4))
            arrived(piece(down * 2 + 1 - c), rs(5))
            arrived(piece(up * 2 + 1 - c), rs(6))
            arrived(piece(far * 2 + 1 - c, 0), rs(7))
            arrived(piece(far * 2 + 1 - c, 1), rs(8))

        def end():
            for i in (0, 1, 4, 5, 6):
                left(piece(t), ss(i))
            left(piece(t, 0), ss(2))
            left(piece(t, 1), ss(3))
            left(piece(t, 0), ss(7))
            left(piece(t, 1), ss(8))

        return one, two, three, four, end

    def chunk_piece(m):
        rows = pl.ds(m * CR, CR)

        def piece(tp, half=None):
            if half is None:
                return xd.at[:, rows, cols(tp)]
            return xd.at[half, rows, cols(tp)]

        return piece

    chunk = [
        gather(
            chunk_piece(m),
            lambda i, m=m: b_send.at[m * 9 + i],
            lambda i, m=m: b_recv.at[m * 9 + i],
        )
        for m in range(CHUNKS)
    ]

    def plane(zz, half=None):
        base = zz * (NX * TOK)
        if half is None:
            return mx.at[pl.ds(pl.multiple_of(base, NX * TOK), NX * TOK), :]
        return mx.at[pl.ds(pl.multiple_of(base + half * 2 * TOK, 2 * TOK), 2 * TOK), :]

    z_up, z_down = ((z + 1) % NZ) * NX + x, ((z + NZ - 1) % NZ) * NX + x

    def hop(r):
        if r == 1:
            for i, (_, _to, source) in enumerate(x_peers):
                arrived(
                    mx.at[pl.ds(pl.multiple_of((z * NX + source) * TOK, TOK), TOK), :],
                    m_recv.at[i],
                )
        else:
            arrived(plane((z + NZ - (r - 1)) % NZ), n_recv.at[2 * r - 2])
            arrived(plane((z + r - 1) % NZ), n_recv.at[2 * r - 1])
        low, high = (0, 1) if r == 4 else (None, None)
        a = plane((z + NZ - (r - 1)) % NZ, low)
        b = plane((z + r - 1) % NZ, high)
        remote(a, a, n_send.at[2 * r], n_recv.at[2 * r], z_up, t).start()
        remote(b, b, n_send.at[2 * r + 1], n_recv.at[2 * r + 1], z_down, t).start()

    for m in range(CHUNKS):
        a_wait(2 * m, 1 if m == 0 else 0)
        a_wait(2 * m + 1, 0)
        chunk[m][0]()
        if m >= 1:
            chunk[m - 1][1]()
        if m >= 2:
            chunk[m - 2][2]()
    hop(1)
    chunk[3][1]()
    chunk[2][2]()
    chunk[3][2]()
    hop(2)
    for m in range(CHUNKS):
        chunk[m][3]()

    for load in loads:
        load.wait()
    half_rows = ROWS // 2
    for m in range(2):
        rows = pl.ds(m * half_rows, half_rows)
        xm = xd[0, rows, :]
        g = dot(xm, wg[...], 1, 0)
        u = dot(xm, wu[...], 1, 0)
        dh = dot(xd[1, rows, :], wd[...], 1, 1)
        sig = 1.0 / (1.0 + jnp.exp(-g))
        act = g * sig
        hid_t[:, rows] = (act * u).T.astype(BF)
        dgu[rows, 0:FFL] = (dh * u * (sig * (1.0 + g * (1.0 - sig)))).astype(BF)
        dgu[rows, OFF : OFF + FFL] = (dh * act).astype(BF)
    hop(3)

    def grads(lo, hi):
        def body(i, carry):
            cs = cols(i)
            gu = dot(xd[0, :, cs], dgu[...], 0, 0)
            og_gate[cs, :] = gu[:, 0:FFL].astype(BF)
            og_up[cs, :] = gu[:, OFF : OFF + FFL].astype(BF)
            og_down[:, cs] = dot(hid_t[...], xd[1, :, cs], 1, 0).astype(BF)
            return carry

        lax.fori_loop(lo, hi, body, 0)

    def dx(m):
        rows = pl.ds(m * CR, CR)
        dg = dgu[rows, 0:FFL]
        du = dgu[rows, OFF : OFF + FFL]

        def body(i, carry):
            cs = cols(i)
            part[i % 2, i // 2, rows, :] = (
                dot(dg, wg[cs, :], 1, 1) + dot(du, wu[cs, :], 1, 1)
            ).astype(BF)
            return carry

        lax.fori_loop(0, 8, body, 0)

    def d_rows(m):
        return pl.ds(m * CR, CR)

    def d_low(m):
        return pl.ds(m * CR, CR // 2)

    def d_high(m):
        return pl.ds(m * CR + CR // 2, CR // 2)

    def d_half(m):
        return pl.ds(m * (CR // 2), CR // 2)

    def d0(m):
        remote(
            part.at[1 - c, :, d_rows(m), :],
            sib.at[:, d_rows(m), :],
            d_send.at[m * 5],
            d_recv.at[m * 5],
            s,
            t_sib,
        ).start()

    def d1(m):
        arrived(sib.at[:, d_rows(m), :], d_recv.at[m * 5])
        ssum[:, d_rows(m), :] = (
            part[c, :, d_rows(m), :].astype(F32) + sib[:, d_rows(m), :].astype(F32)
        ).astype(BF)
        remote(
            ssum.at[far, d_low(m), :],
            rl.at[d_half(m), :],
            d_send.at[m * 5 + 1],
            d_recv.at[m * 5 + 1],
            s,
            t_up,
        ).start()
        remote(
            ssum.at[far, d_high(m), :],
            rr.at[d_half(m), :],
            d_send.at[m * 5 + 2],
            d_recv.at[m * 5 + 2],
            s,
            t_down,
        ).start()

    def d2(m):
        arrived(rl.at[d_half(m), :], d_recv.at[m * 5 + 1])
        ssum[up, d_low(m), :] = (
            ssum[up, d_low(m), :].astype(F32) + rl[d_half(m), :].astype(F32)
        ).astype(BF)
        remote(
            ssum.at[up, d_rows(m), :],
            fl.at[d_rows(m), :],
            d_send.at[m * 5 + 3],
            d_recv.at[m * 5 + 3],
            s,
            t_up,
        ).start()
        arrived(rr.at[d_half(m), :], d_recv.at[m * 5 + 2])
        ssum[down, d_high(m), :] = (
            ssum[down, d_high(m), :].astype(F32) + rr[d_half(m), :].astype(F32)
        ).astype(BF)
        remote(
            ssum.at[down, d_rows(m), :],
            fr.at[d_rows(m), :],
            d_send.at[m * 5 + 4],
            d_recv.at[m * 5 + 4],
            s,
            t_down,
        ).start()

    def e_copy(k, xx):
        target = ((z + NZ - offset_of(k)) % NZ) * NX + xx
        i = k * NX + xx
        return remote(
            rsum.at[pl.ds(pl.multiple_of(i * CAP, CAP), CAP), :],
            ret.at[pl.ds(pl.multiple_of(s * CAP, CAP), CAP), :],
            e_send.at[i],
            e_recv.at[s],
            target,
            t,
        )

    def d3(m):
        arrived(fl.at[d_rows(m), :], d_recv.at[m * 5 + 3])
        arrived(fr.at[d_rows(m), :], d_recv.at[m * 5 + 4])
        rsum[d_rows(m), :] = (
            ssum[y, d_rows(m), :].astype(F32)
            + fl[d_rows(m), :].astype(F32)
            + fr[d_rows(m), :].astype(F32)
        ).astype(BF)

        def start(k, first):
            def body(i, carry):
                e_copy(k, (x + i) % NX).start()
                return carry

            lax.fori_loop(first, NX, body, 0)

        start(2 * m + 1, 0)
        start(2 * m, 1 if m == 0 else 0)
        if m == 0:
            ret[pl.ds(pl.multiple_of(s * CAP, CAP), CAP), :] = rsum[here, :]

    dx(3)
    d0(3)
    dx(2)
    d0(2)
    d1(3)
    dx(1)
    d0(1)
    d1(2)
    d2(3)
    dx(0)
    d0(0)
    d1(1)
    d2(2)
    grads(0, 2)
    d3(3)
    d1(0)
    d2(1)
    grads(2, 4)
    d3(2)
    d2(0)
    hop(4)
    d3(1)
    grads(4, 6)
    d3(0)
    grads(6, 8)
    stores = [
        pltpu.make_async_copy(og_gate, g_gate.at[0], o_sem.at[0]),
        pltpu.make_async_copy(og_up, g_up.at[0], o_sem.at[1]),
        pltpu.make_async_copy(og_down, g_down.at[0], o_sem.at[2]),
    ]
    for store in stores:
        store.start()

    def e_wait(i, carry):
        e = (s + i) % NSP
        arrived(ret.at[pl.ds(pl.multiple_of(e * CAP, CAP), CAP), :], e_recv.at[e])
        return carry

    lax.fori_loop(1, NSP, e_wait, 0)

    dh = out_grad[...].astype(F32) + dot(place[...], ret[...], 0, 0)
    js[...] = dh.T.astype(BF)
    hf[:, cols(t)] = dh.astype(BF)

    own_cols = pl.ds(pl.multiple_of(s * TOK, TOK), TOK)
    for j in range(NX):
        mine = jnp.logical_and(z == t, x == j)

        @pl.when(jnp.logical_not(mine))
        def _():
            remote(
                js.at[pl.ds(64 * j, 64), :],
                dt.at[:, own_cols],
                j_send.at[j],
                j_recv.at[x],
                t * NX + j,
                z,
            ).start()

        @pl.when(mine)
        def _():
            dt[:, own_cols] = js[pl.ds(64 * j, 64), :]

    def h_piece(tp, half=None):
        if half is None:
            return hf.at[:, cols(tp)]
        return hf.at[pl.ds(half * 64, 64), cols(tp)]

    def j_piece(tp, half=None):
        if half is None:
            return dt.at[:, cols(tp, 512)]
        return dt.at[pl.ds(half * 32, 32), cols(tp, 512)]

    hg = gather(h_piece, lambda i: h_send.at[i], lambda i: h_recv.at[i])
    jg = gather(j_piece, lambda i: k_send.at[i], lambda i: k_recv.at[i])
    hg[0]()
    hg[1]()
    for j in range(NX):

        @pl.when(jnp.logical_not(jnp.logical_and(z == t, x == j)))
        def _():
            arrived(
                dt.at[:, pl.ds(pl.multiple_of(t * 512 + j * TOK, TOK), TOK)], j_recv.at[j]
            )

    jg[0]()
    hg[2]()
    hg[3]()
    dz = dot(hf[...], wo[...], 1, 0)
    dconv = (dz * gate_b[...].astype(F32)).astype(BF)
    hsend[...] = dconv

    @pl.when(s < NSP - 1)
    def _():
        remote(
            hsend.at[pl.ds(TOK - 16, 16), :], halo.at[0], j_send.at[4], j_recv.at[4], s + 1, t
        ).start()

    @pl.when(s > 0)
    def _():
        remote(hsend.at[pl.ds(0, 16), :], halo.at[1], j_send.at[5], j_recv.at[5], s - 1, t).start()

    jg[1]()
    g_b[...] = (dz * conv_out[...].astype(F32)).astype(BF)
    jg[2]()

    @pl.when(s > 0)
    def _():
        arrived(halo.at[0], j_recv.at[4])

    @pl.when(s == 0)
    def _():
        halo[0] = jnp.zeros((16, CH), BF)

    @pl.when(s < NSP - 1)
    def _():
        arrived(halo.at[1], j_recv.at[5])

    @pl.when(s == NSP - 1)
    def _():
        halo[1] = jnp.zeros((16, CH), BF)

    d = dconv.astype(F32)
    at_row = lax.broadcasted_iota(jnp.int32, (TOK, CH), 0)
    before_first = halo[0].astype(F32)[15:16, :]
    after_last = halo[1].astype(F32)[0:1, :]
    earlier_rows = jnp.where(at_row == 0, before_first, pltpu.roll(d, 1, 0))
    later_rows = jnp.where(at_row == TOK - 1, after_last, pltpu.roll(d, TOK - 1, 0))
    tp3 = taps[...]
    grad_u = tp3[0:1, :] * later_rows + tp3[1:2, :] * d + tp3[2:3, :] * earlier_rows
    g_c[...] = (grad_u * value_v[...].astype(F32)).astype(BF)
    g_v[...] = (grad_u * gate_c[...].astype(F32)).astype(BF)

    arrived(plane((z + 4) % NZ, 0), n_recv.at[8])
    arrived(plane((z + 4) % NZ, 1), n_recv.at[9])
    jg[3]()
    g_out[...] = dot(dt[...], mx[...], 1, 0)

    def a_left(i, carry):
        a_copy(i).wait_send()
        return carry

    lax.fori_loop(1, NSP, a_left, 0)
    for m in range(CHUNKS):
        chunk[m][4]()
        left(part.at[0, :, d_rows(m), :], d_send.at[m * 5])
        left(rl.at[d_half(m), :], d_send.at[m * 5 + 1])
        left(rr.at[d_half(m), :], d_send.at[m * 5 + 2])
        left(fl.at[d_rows(m), :], d_send.at[m * 5 + 3])
        left(fr.at[d_rows(m), :], d_send.at[m * 5 + 4])

    def e_left(i, carry):
        e_copy(i // NX, (x + i % NX) % NX).wait_send()
        return carry

    lax.fori_loop(1, NSP, e_left, 0)
    hg[4]()
    jg[4]()
    for i in range(3):
        left(mx.at[own_rows, :], m_send.at[i])
    for r in range(1, 5):
        half = 0 if r == 4 else None
        left(plane(z, half), n_send.at[2 * r])
        left(plane(z, half), n_send.at[2 * r + 1])
    for j in range(NX):

        @pl.when(jnp.logical_not(jnp.logical_and(z == t, x == j)))
        def _():
            left(js.at[pl.ds(64 * j, 64), :], j_send.at[j])

    @pl.when(s < NSP - 1)
    def _():
        left(halo.at[0], j_send.at[4])

    @pl.when(s > 0)
    def _():
        left(halo.at[1], j_send.at[5])

    for store in stores:
        store.wait()


def local(
    out_grad,
    moe_input,
    route_weight,
    route_ids,
    gate_proj,
    up_proj,
    down_proj,
    out_proj,
    conv_out,
    gate_b,
    gate_c,
    value_v,
    conv_taps,
):
    vm = pl.BlockSpec(memory_space=pltpu.VMEM)
    hbm = pl.BlockSpec(memory_space=pl.ANY)
    dma = pltpu.SemaphoreType.DMA
    shape = jax.ShapeDtypeStruct
    return pl.pallas_call(
        kernel,
        out_shape=(
            shape((1, D, FFL), BF),
            shape((1, D, FFL), BF),
            shape((1, FFL, D), BF),
            shape((64, CH), F32),
            shape((TOK, CH), BF),
            shape((TOK, CH), BF),
            shape((TOK, CH), BF),
        ),
        in_specs=[vm, vm, vm, vm, hbm, hbm, hbm, hbm, vm, vm, vm, vm, vm],
        out_specs=(hbm, hbm, hbm, vm, vm, vm, vm),
        scratch_shapes=[
            pltpu.VMEM((2, ROWS, CH), BF),
            pltpu.VMEM((2, ROWS, D), BF),
            pltpu.VMEM((D, FFL), BF),
            pltpu.VMEM((D, FFL), BF),
            pltpu.VMEM((FFL, D), BF),
            pltpu.VMEM((D, CH), BF),
            pltpu.VMEM((ROWS, TOK), BF),
            pltpu.VMEM((ROWS, 2 * OFF), BF),
            pltpu.VMEM((FFL, ROWS), BF),
            pltpu.VMEM((2, NY, ROWS, CH), BF),
            pltpu.VMEM((NY, ROWS, CH), BF),
            pltpu.VMEM((NY, ROWS, CH), BF),
            pltpu.VMEM((ROWS // 2, CH), BF),
            pltpu.VMEM((ROWS // 2, CH), BF),
            pltpu.VMEM((ROWS, CH), BF),
            pltpu.VMEM((ROWS, CH), BF),
            pltpu.VMEM((ROWS, CH), BF),
            pltpu.VMEM((ROWS, CH), BF),
            pltpu.VMEM((TOK, D), BF),
            pltpu.VMEM((CH, TOK), BF),
            pltpu.VMEM((64, NSP * TOK), BF),
            pltpu.VMEM((NSP * TOK, CH), BF),
            pltpu.VMEM((TOK, CH), BF),
            pltpu.VMEM((2, 16, CH), BF),
            pltpu.VMEM((D, FFL), BF),
            pltpu.VMEM((D, FFL), BF),
            pltpu.VMEM((FFL, D), BF),
            dma((4,)),
            dma((3,)),
            dma((NSP,)),
            dma((NSP,)),
            dma((9 * CHUNKS,)),
            dma((9 * CHUNKS,)),
            dma((5 * CHUNKS,)),
            dma((5 * CHUNKS,)),
            dma((NSP,)),
            dma((NSP,)),
            dma((9,)),
            dma((9,)),
            dma((6,)),
            dma((6,)),
            dma((9,)),
            dma((9,)),
            dma((3,)),
            dma((3,)),
            dma((10,)),
            dma((10,)),
        ],
        compiler_params=pltpu.CompilerParams(
            collective_id=0, has_side_effects=True, vmem_limit_bytes=60 * 1024 * 1024
        ),
        name="layer",
    )(
        out_grad,
        moe_input,
        route_weight,
        route_ids.T,
        gate_proj,
        up_proj,
        down_proj,
        out_proj,
        conv_out,
        gate_b,
        gate_c,
        value_v,
        conv_taps,
    )


def solution(mesh):
    return jax.shard_map(
        local,
        mesh=mesh,
        in_specs=(
            P("sp", "tp"),
            P("sp", "tp"),
            P("sp", None),
            P("sp", None),
            P("sp", None, "tp"),
            P("sp", None, "tp"),
            P("sp", "tp", None),
            P(None, "tp"),
            P("sp", "tp"),
            P("sp", "tp"),
            P("sp", "tp"),
            P("sp", "tp"),
            P(None, "tp"),
        ),
        out_specs=(
            P("sp", None, "tp"),
            P("sp", None, "tp"),
            P("sp", "tp", None),
            P("sp", "tp"),
            P("sp", "tp"),
            P("sp", "tp"),
            P("sp", "tp"),
        ),
        check_vma=False,
    )
```

time: 292 us -> 109 us (0.37); the launches traced: 286 us -> 108 us
  waiting for transfers between devices: 145 us -> 0 us
  Pallas kernels: 0 us -> 94.3 us
  blocking collectives: 72.9 us -> 0 us
  matrix products: 16.7 us -> 0 us
  starting transfers between devices: 15.1 us -> 0 us
  between operations: 14.2 us -> 0.67 us
  other arithmetic: 8.14 us -> 0 us
    reduce_scatter x4 -> x0, waiting for transfers between devices: 97.7 us -> none  [own_block(): blocks = lax.psum_scatter(blocks, axes[k], scatter_dimension=0, tiled=True)]
    pallas_call x0 -> x1, Pallas kernels: none -> 94.3 us  [local(): pl.pallas_call(kernel, out_shape=(shape((1, D, FFL), BF), shape((1, D, FF...]
    all_to_all x3 -> x0, blocking collectives: 72.9 us -> none  [the longest x1 30.2 us: summed_on_arrival(): lax.all_to_all(blocks, axis, split_axis=0, concat_axis=0, tiled=True)]
    all_gather x1 -> x0, waiting for transfers between devices: 36.7 us -> none  [in_one_piece(): lax.all_gather(both, axis, axis=dim, tiled=True)]
    dot_general x10 -> x0, matrix products: 16.7 us -> none  [the longest x1 3.76 us: local(): jnp.dot(xin.T, dgate, preferred_element_type=jnp.float32)]
    all_to_all x1 -> x0, waiting for transfers between devices: 10.5 us -> none  [local(): lax.all_to_all(summed.reshape(n_experts, capacity, local_cols), SP, split...]
    all_to_all x1 -> x0, starting transfers between devices: 9.67 us -> none  [local(): lax.all_to_all(summed.reshape(n_experts, capacity, local_cols), SP, split...]
    unnamed x44 -> x22, local copies, waits for them, and re-layouts: 3.7 us -> 9.31 us
  transfers between devices with their start and end apart: 8 -> 0, of which waited for: 6 -> 0; matrix products, arithmetic and copies ran while one was open for 4% -> 0% of each run, Pallas kernels for 0% -> 0%
where the time goes in v1:
time: 109 us; the launch traced here: 108 us
  Pallas kernels  94.3 us (87%)
  local copies, waits for them, and re-layouts  13.5 us (12%)
    pallas_call x1, Pallas kernels, local(): pl.pallas_call(kernel, out_shape=(shape((1, D, FFL), BF), shape((1, D, FF...  94.3 us
    unnamed x22, local copies, waits for them, and re-layouts  9.31 us
    pallas_call x2, local copies, waits for them, and re-layouts, local(): pl.pallas_call(kernel, out_shape=(shape((1, D, FFL), BF), shape((1, D, FF...  4.24 us

profile of v1, /device:TPU:1, one launch (start us, length us, event | category | flops | bytes accessed | tf_op | source)
XLA Modules:
  0.0 108.5 jit_solution(4906386498846433441)
XLA Ops:
  0.6 1.4 %copy.20.route_weight = f32[128,2]{1,0:T(8,128)} copy(f32[128,2]{0,1:T(2,128)} %param.15) | data formatting | bytes 2048 | tf_op args[2]
  2.0 0.0 copy-start.1
  2.0 2.7 %copy.21.gate_proj = bf16[1,2048,352]{2,1,0:T(8,128)(2,1)} copy(bf16[1,2048,352]{1,2,0:T(8,128)(2,1)} %param.17) | data formatting | bytes 2883584 | tf_op args[4]
  4.7 0.0 copy-done.1
  4.7 1.6 %copy.22.up_proj = bf16[1,2048,352]{2,1,0:T(8,128)(2,1)} copy(bf16[1,2048,352]{1,2,0:T(8,128)(2,1)S(1)} %copy-done.1) | data formatting | bytes 2883584 | tf_op args[5]
  6.3 94.3 %layer.1 = (bf16[1,2048,352]{2,1,0:T(8,128)(2,1)}, bf16[1,2048,352]{2,1,0:T(8,128)(2,1)}, bf16[1,352,2048]{2,1,0:T(8,128)(2,1)}, f32[64,256]{1,0:T(8,128)}, bf16...) custom-call(bf16[128,256]{1,0:T(8,128)(2,1)} %out_grad.1, bf16[128,256]{1,0:T(8,128)(2,1)} %moe_input.1, ...), custom_call_target="tpu_custom_call" | custom-call | tf_op jit(solution)/shard_map/layer/pallas_call | solution.py:658
  100.6 0.0 copy-start
  100.6 2.7 %copy.23 = bf16[1,2048,352]{1,2,0:T(8,128)(2,1)} copy(bf16[1,2048,352]{2,1,0:T(8,128)(2,1)} %get-tuple-element.7) | data formatting | bytes 2883584 | tf_op jit(solution)/shard_map/layer/pallas_call | solution.py:658
  103.2 0.0 copy-done
  103.2 0.0 copy-start.2
  103.2 1.6 %copy.24 = bf16[1,2048,352]{1,2,0:T(8,128)(2,1)} copy(bf16[1,2048,352]{2,1,0:T(8,128)(2,1)S(1)} %copy-done) | data formatting | bytes 2883584 | tf_op jit(solution)/shard_map/layer/pallas_call | solution.py:658
  104.8 0.0 copy-done.2
  104.8 0.0 copy-start.6
  104.8 0.0 copy-start.5
  104.8 0.0 copy-start.3
  104.8 1.1 %copy.30 = bf16[1,352,2048]{2,1,0:T(8,128)(2,1)} copy(bf16[1,352,2048]{2,1,0:T(8,128)(2,1)S(1)} %copy-done.2) | data formatting | bytes 2883584
  106.0 0.0 copy-done.6
  106.0 0.6 copy.31
  106.6 0.0 copy-done.5
  106.6 0.6 copy.32
  107.2 0.0 copy-done.4
  107.2 0.6 copy.33
  107.8 0.0 copy-done.3
  107.9 0.6 copy.34
  (1 shorter events, 0.0 us)
Async XLA Ops:
  2.0 2.7 %copy-start.1 = (bf16[1,2048,352]{1,2,0:T(8,128)(2,1)S(1)}, bf16[1,2048,352]{1,2,0:T(8,128)(2,1)}, u32[]{:S(2)}) copy-start(bf16[1,2048,352]{1,2,0:T(8,128)(2,1)} %param.18) | copy-start | bytes 4325380
  100.6 2.7 %copy-start = (bf16[1,2048,352]{2,1,0:T(8,128)(2,1)S(1)}, bf16[1,2048,352]{2,1,0:T(8,128)(2,1)}, u32[]{:S(2)}) copy-start(bf16[1,2048,352]{2,1,0:T(8,128)(2,1)} %get-tuple-element.8) | copy-start | bytes 4325380
  103.2 1.6 %copy-start.2 = (bf16[1,352,2048]{2,1,0:T(8,128)(2,1)S(1)}, bf16[1,352,2048]{2,1,0:T(8,128)(2,1)}, u32[]{:S(2)}) copy-start(bf16[1,352,2048]{2,1,0:T(8,128)(2,1)} %get-tuple-element.23) | copy-start | bytes 4325380
  104.8 1.1 %copy-start.6 = (f32[64,256]{1,0:T(8,128)S(1)}, f32[64,256]{1,0:T(8,128)}, u32[]{:S(2)}) copy-start(f32[64,256]{1,0:T(8,128)} %get-tuple-element.24) | copy-start | bytes 196612
  104.8 1.8 %copy-start.5 = (bf16[128,256]{1,0:T(8,128)(2,1)S(1)}, bf16[128,256]{1,0:T(8,128)(2,1)}, u32[]{:S(2)}) copy-start(bf16[128,256]{1,0:T(8,128)(2,1)} %get-tuple-element.25) | copy-start | bytes 196612
  104.8 2.4 %copy-start.4 = (bf16[128,256]{1,0:T(8,128)(2,1)S(1)}, bf16[128,256]{1,0:T(8,128)(2,1)}, u32[]{:S(2)}) copy-start(bf16[128,256]{1,0:T(8,128)(2,1)} %get-tuple-element.26) | copy-start | bytes 196612
  104.8 3.0 %copy-start.3 = (bf16[128,256]{1,0:T(8,128)(2,1)S(1)}, bf16[128,256]{1,0:T(8,128)(2,1)}, u32[]{:S(2)}) copy-start(bf16[128,256]{1,0:T(8,128)(2,1)} %get-tuple-element.27) | copy-start | bytes 196612

commit v2 on v1

v2 whole, which is shorter than its diff:
```python
import jax
import jax.numpy as jnp
from jax import lax
from jax.experimental import pallas as pl
from jax.experimental.pallas import tpu as pltpu
from jax.sharding import PartitionSpec as P

MESH = pl.DeviceIdType.MESH
BF = jnp.bfloat16
F32 = jnp.float32
NZ, NX, NY = 8, 4, 4
NSP = NZ * NX
CAP = 16
TOK = 128
CH = 256
D = 2048
FFL = 352
ROWS = NSP * CAP
NK = 8
CR = ROWS // NK
NP = 4
PR = ROWS // NP
ORDER = (0, 1, 7, 4, 3, 5, 2, 6)


def dot(a, b, ca, cb):
    return lax.dot_general(a, b, (((ca,), (cb,)), ((), ())), preferred_element_type=F32)


def kernel(
    out_grad_h,
    moe_input_h,
    weight_h,
    ids_h,
    gate_proj,
    up_proj,
    down_proj,
    out_proj_h,
    conv_out_h,
    gate_b_h,
    gate_c_h,
    value_v_h,
    taps_h,
    g_gate,
    g_up,
    g_down,
    g_out_h,
    g_b_h,
    g_c_h,
    g_v_h,
    out_grad,
    moe_input,
    weight_t,
    ids_t,
    out_proj,
    conv_out,
    gate_b,
    gate_c,
    value_v,
    taps,
    g_out,
    g_b,
    g_c,
    g_v,
    og_gu,
    og_down,
    i_sem,
    o_sem,
    send,
    xd,
    wgu,
    wd,
    place,
    dgu_t,
    hid_t,
    part,
    sib,
    ssum,
    along,
    rsum,
    ret,
    hf,
    js,
    dt,
    mx,
    hsend,
    halo,
    w_sem,
    a_send,
    a_recv,
    b_send,
    b_recv,
    d_send,
    d_recv,
    e_send,
    e_recv,
    h_send,
    h_recv,
    j_send,
    j_recv,
    k_send,
    k_recv,
    m_send,
    m_recv,
    n_send,
    n_recv,
):
    s = lax.axis_index("sp")
    t = lax.axis_index("tp")
    z, x = s // NX, s % NX
    y, c = t // 2, t % 2
    up, down, far = (y + 1) % NY, (y + NY - 1) % NY, (y + 2) % NY
    t_up, t_down, t_sib = up * 2 + c, down * 2 + c, y * 2 + (1 - c)
    t_far = far * 2 + c

    def remote(src, dst, ssem, rsem, sp, tp):
        return pltpu.make_async_remote_copy(
            src_ref=src,
            dst_ref=dst,
            send_sem=ssem,
            recv_sem=rsem,
            device_id={"sp": sp, "tp": tp},
            device_id_type=MESH,
        )

    def arrived(ref, rsem):
        remote(ref, ref, n_send.at[0], rsem, s, t).wait_recv()

    def left(ref, ssem):
        remote(ref, ref, ssem, n_recv.at[0], s, t).wait_send()

    barrier = pltpu.get_barrier_semaphore()

    def greet(i, carry):
        pl.semaphore_signal(
            barrier, inc=1, device_id={"sp": (s + i) % NSP, "tp": t}, device_id_type=MESH
        )
        return carry

    lax.fori_loop(1, NSP, greet, 0)
    for peer in (t_up, t_down, t_far, t_sib):
        pl.semaphore_signal(barrier, inc=1, device_id={"sp": s, "tp": peer}, device_id_type=MESH)
    for j in range(NX):

        @pl.when(jnp.logical_not(jnp.logical_and(z == t, x == j)))
        def _():
            pl.semaphore_signal(
                barrier, inc=1, device_id={"sp": t * NX + j, "tp": z}, device_id_type=MESH
            )

    small = [
        pltpu.make_async_copy(a, b, i_sem.at[i])
        for i, (a, b) in enumerate(
            (
                (ids_h, ids_t),
                (weight_h, weight_t),
                (out_grad_h, out_grad),
                (moe_input_h, moe_input),
                (gate_b_h, gate_b),
                (conv_out_h, conv_out),
                (gate_c_h, gate_c),
                (value_v_h, value_v),
                (taps_h, taps),
                (out_proj_h, out_proj),
            )
        )
    ]
    loads = [
        pltpu.make_async_copy(gate_proj.at[0], wgu.at[pl.ds(0, FFL), :], w_sem.at[0]),
        pltpu.make_async_copy(up_proj.at[0], wgu.at[pl.ds(FFL, FFL), :], w_sem.at[1]),
        pltpu.make_async_copy(down_proj.at[0], wd, w_sem.at[2]),
    ]
    for load in small:
        load.start()
    for load in loads:
        load.start()

    for load in small[:6]:
        load.wait()

    ids = ids_t[...]
    experts = lax.broadcasted_iota(jnp.int32, (NSP, TOK), 0)
    e0 = jnp.where(experts == ids[0:1, :], 1.0, 0.0).astype(F32)
    e1 = jnp.where(experts == ids[1:2, :], 1.0, 0.0).astype(F32)
    row = lax.broadcasted_iota(jnp.int32, (TOK, TOK), 0)
    col = lax.broadcasted_iota(jnp.int32, (TOK, TOK), 1)
    earlier = jnp.where(row < col, 1.0, 0.0).astype(BF)
    before = dot((e0 + e1).astype(BF), earlier, 1, 0)
    slot0 = jnp.sum(before * e0, axis=0, keepdims=True)
    slot1 = jnp.sum(before * e1, axis=0, keepdims=True)
    idf = ids.astype(F32) * CAP
    at = lax.broadcasted_iota(jnp.int32, (ROWS, TOK), 0).astype(F32)
    p0 = jnp.where(at == idf[0:1, :] + slot0, 1.0, 0.0).astype(BF)
    p1 = jnp.where(at == idf[1:2, :] + slot1, 1.0, 0.0).astype(BF)
    place[...] = p0 + p1
    og = out_grad[...].astype(F32)
    w = weight_t[...]
    w0 = jnp.broadcast_to(w[0:1, :], (TOK, TOK)).T
    w1 = jnp.broadcast_to(w[1:2, :], (TOK, TOK)).T
    dy0 = (jnp.concatenate([w0, w0], axis=1) * og).astype(BF)
    dy1 = (jnp.concatenate([w1, w1], axis=1) * og).astype(BF)
    send[0] = dot(p0 + p1, moe_input[...], 1, 0).astype(BF)
    send[1] = (dot(p0, dy0, 1, 0) + dot(p1, dy1, 1, 0)).astype(BF)
    mixed = (gate_b[...].astype(F32) * conv_out[...].astype(F32)).astype(BF)
    own_rows = pl.ds(pl.multiple_of(s * TOK, TOK), TOK)
    mx[own_rows, :] = mixed

    def cols(tp, width=CH):
        return pl.ds(pl.multiple_of(tp * width, width), width)

    pl.semaphore_wait(barrier, NSP - 1 + 4 + 4 - jnp.where(z == t, 1, 0))

    def a_copy(k, xx):
        target = ((z + ORDER[k]) % NZ) * NX + xx
        src = send.at[:, pl.ds(pl.multiple_of(target * CAP, CAP), CAP), :]
        dst = xd.at[:, pl.ds(pl.multiple_of(k * CR + x * CAP, CAP), CAP), cols(t)]
        return remote(src, dst, a_send.at[k * NX + xx], a_recv.at[k * NX + x], target, t)

    def each_x(first, do):
        def body(i, carry):
            do((x + i) % NX)
            return carry

        lax.fori_loop(first, NX, body, 0)

    def a_start(k):
        each_x(1 if k == 0 else 0, lambda xx: a_copy(k, xx).start())

    def a_wait(k):
        def one(xx):
            arrived(
                xd.at[:, pl.ds(pl.multiple_of(k * CR + xx * CAP, CAP), CAP), cols(t)],
                a_recv.at[k * NX + xx],
            )

        each_x(1 if k == 0 else 0, one)

    here = pl.ds(pl.multiple_of(x * CAP, CAP), CAP)

    def gather(piece, ss, rs):
        def one():
            for i, peer in enumerate((t_sib, t_up, t_down, t_far)):
                remote(piece(t), piece(t), ss(i), rs(i), s, peer).start()

        def two():
            for i, origin in enumerate((t_down, t_up, t_far)):
                arrived(piece(origin), rs(1 + i))
                remote(piece(origin), piece(origin), ss(4 + i), rs(4 + i), s, t_sib).start()

        def three():
            for i, origin in enumerate((y, down, up, far)):
                arrived(piece(origin * 2 + 1 - c), rs(i if i == 0 else 3 + i))

        def end():
            for i in range(7):
                left(piece(t), ss(i))

        return one, two, three, end

    def relay(piece, ss, rs):
        def one():
            for i, peer in enumerate((t_sib, t_up, t_down)):
                remote(piece(t), piece(t), ss(i), rs(i), s, peer).start()

        def two():
            for i, (origin, peer) in enumerate(((t_down, t_up), (t_up, t_down))):
                arrived(piece(origin), rs(1 + i))
                half = piece(origin, i)
                remote(half, half, ss(3 + i), rs(3 + i), s, peer).start()
                remote(piece(origin), piece(origin), ss(5 + i), rs(5 + i), s, t_sib).start()

        def three():
            for i in range(2):
                half = piece(t_far, i)
                arrived(half, rs(3 + i))
                remote(half, half, ss(7 + i), rs(7 + i), s, t_sib).start()

        def four():
            arrived(piece(t_sib), rs(0))
            arrived(piece(down * 2 + 1 - c), rs(5))
            arrived(piece(up * 2 + 1 - c), rs(6))
            arrived(piece(far * 2 + 1 - c, 0), rs(7))
            arrived(piece(far * 2 + 1 - c, 1), rs(8))

        def end():
            for i in range(9):
                left(piece(t) if i in (0, 1, 2, 5, 6) else piece(t, 0), ss(i))

        return one, two, three, four, end

    def chunk_piece(k):
        rows = pl.ds(k * CR, CR)

        def piece(tp, half=None):
            if half is None:
                return xd.at[:, rows, cols(tp)]
            return xd.at[half, rows, cols(tp)]

        return piece

    chunk = [
        relay(
            chunk_piece(k),
            lambda i, k=k: b_send.at[k * 9 + i],
            lambda i, k=k: b_recv.at[k * 9 + i],
        )
        for k in range(NK)
    ]

    def block(zz, xx, half=None):
        base = (zz * NX + xx) * TOK
        if half is None:
            return mx.at[pl.ds(pl.multiple_of(base, TOK), TOK), :]
        return mx.at[pl.ds(pl.multiple_of(base + half * (TOK // 2), TOK // 2), TOK // 2), :]

    z_up, z_down = ((z + 1) % NZ) * NX + x, ((z + NZ - 1) % NZ) * NX + x
    x_up, x_down, x_far = (x + 1) % NX, (x + NX - 1) % NX, (x + 2) % NX

    def z_hop(r):
        low, high = (0, 1) if r == 4 else (None, None)
        a = block((z + NZ - (r - 1)) % NZ, x, low)
        b = block((z + r - 1) % NZ, x, high)
        remote(a, a, n_send.at[2 * r], n_recv.at[2 * r], z_up, t).start()
        remote(b, b, n_send.at[2 * r + 1], n_recv.at[2 * r + 1], z_down, t).start()

    def z_arrived(r):
        low, high = (0, 1) if r == 4 else (None, None)
        arrived(block((z + NZ - r) % NZ, x, low), n_recv.at[2 * r])
        arrived(block((z + r) % NZ, x, high), n_recv.at[2 * r + 1])

    def x_hop(d):
        a = block((z + d) % NZ, x)
        for i, to in enumerate((x_up, x_down, x_far)):
            remote(a, a, m_send.at[3 * d + i], m_recv.at[3 * d + i], z * NX + to, t).start()

    def forward(lo, hi):
        rows = pl.ds(lo * CR, (hi - lo) * CR)
        gu = dot(wgu[...], xd[0, rows, :], 1, 1)
        dh = dot(wd[...], xd[1, rows, :], 1, 1)
        g, u = gu[:FFL], gu[FFL:]
        sig = 1.0 / (1.0 + jnp.exp(-g))
        act = g * sig
        hid_t[:, rows] = (act * u).astype(BF)
        dgu_t[0:FFL, rows] = (dh * u * (sig * (1.0 + g * (1.0 - sig)))).astype(BF)
        dgu_t[FFL : 2 * FFL, rows] = (dh * act).astype(BF)

    def grads(lo, hi):
        def body(i, carry):
            cs = cols(i)
            og_gu[:, cs] = dot(dgu_t[...], xd[0, :, cs], 1, 0).astype(BF)
            og_down[:, cs] = dot(hid_t[...], xd[1, :, cs], 1, 0).astype(BF)
            return carry

        lax.fori_loop(lo, hi, body, 0)

    def dx(m):
        rows = pl.ds(m * PR, PR)
        dg = dgu_t[:, rows].T

        def body(i, carry):
            part[i % 2, i // 2, rows, :] = dot(dg, wgu[:, cols(i)], 1, 0).astype(BF)
            return carry

        lax.fori_loop(0, 8, body, 0)

    def d_rows(m):
        return pl.ds(m * PR, PR)

    def d0(m):
        remote(
            part.at[1 - c, :, d_rows(m), :],
            sib.at[:, d_rows(m), :],
            d_send.at[m * 4],
            d_recv.at[m * 4],
            s,
            t_sib,
        ).start()

    def d1(m):
        arrived(sib.at[:, d_rows(m), :], d_recv.at[m * 4])
        ssum[:, d_rows(m), :] = (
            part[c, :, d_rows(m), :].astype(F32) + sib[:, d_rows(m), :].astype(F32)
        ).astype(BF)
        for i, (to, peer) in enumerate(((far, t_far), (up, t_up), (down, t_down))):
            remote(
                ssum.at[to, d_rows(m), :],
                along.at[i, d_rows(m), :],
                d_send.at[m * 4 + 1 + i],
                d_recv.at[m * 4 + 1 + i],
                s,
                peer,
            ).start()

    def e_copy(k, xx):
        target = ((z + NZ - ORDER[k]) % NZ) * NX + xx
        i = k * NX + xx
        return remote(
            rsum.at[pl.ds(pl.multiple_of(i * CAP, CAP), CAP), :],
            ret.at[pl.ds(pl.multiple_of(s * CAP, CAP), CAP), :],
            e_send.at[i],
            e_recv.at[s],
            target,
            t,
        )

    def d3(m):
        for i in range(3):
            arrived(along.at[i, d_rows(m), :], d_recv.at[m * 4 + 1 + i])
        rsum[d_rows(m), :] = (
            ssum[y, d_rows(m), :].astype(F32)
            + along[0, d_rows(m), :].astype(F32)
            + along[1, d_rows(m), :].astype(F32)
            + along[2, d_rows(m), :].astype(F32)
        ).astype(BF)
        for k in (2 * m, 2 * m + 1):
            each_x(1 if k == 0 else 0, lambda xx: e_copy(k, xx).start())
        if m == 0:
            ret[pl.ds(pl.multiple_of(s * CAP, CAP), CAP), :] = rsum[here, :]

    z_hop(1)
    for k in range(NK):
        a_start(k)
    xd[:, here, cols(t)] = send[:, pl.ds(pl.multiple_of(s * CAP, CAP), CAP), :]
    x_hop(0)
    for k in range(NK):
        a_wait(k)
        chunk[k][0]()
        if k >= 1:
            chunk[k - 1][1]()
        if k >= 2:
            chunk[k - 2][2]()
        if k == 3:
            z_arrived(1)
            z_hop(2)
            x_hop(1)
            x_hop(7)
        if k == 5:
            z_arrived(2)
            z_hop(3)
            x_hop(2)
            x_hop(6)
    for k in range(4):
        chunk[k][3]()
    for load in loads:
        load.wait()
    forward(0, 4)
    chunk[7][1]()
    chunk[6][2]()
    dx(0)
    d0(0)
    chunk[7][2]()
    z_arrived(3)
    z_hop(4)
    x_hop(3)
    x_hop(5)
    dx(1)
    d0(1)
    d1(0)
    chunk[4][3]()
    chunk[5][3]()
    forward(4, 6)
    d1(1)
    dx(2)
    d0(2)
    d3(0)
    chunk[6][3]()
    chunk[7][3]()
    forward(6, 8)
    d1(2)
    dx(3)
    d0(3)
    z_arrived(4)
    x_hop(4)
    d3(1)
    grads(0, 1)
    d1(3)
    d3(2)
    grads(1, 4)
    d3(3)
    grads(4, 8)
    stores = [
        pltpu.make_async_copy(og_gu.at[pl.ds(0, FFL), :], g_gate.at[0], o_sem.at[0]),
        pltpu.make_async_copy(og_gu.at[pl.ds(FFL, FFL), :], g_up.at[0], o_sem.at[1]),
        pltpu.make_async_copy(og_down, g_down.at[0], o_sem.at[2]),
    ]
    for store in stores:
        store.start()
    for load in small[6:]:
        load.wait()

    def e_wait(i, carry):
        e = (s + i) % NSP
        arrived(ret.at[pl.ds(pl.multiple_of(e * CAP, CAP), CAP), :], e_recv.at[e])
        return carry

    lax.fori_loop(1, NSP, e_wait, 0)

    dh = out_grad[...].astype(F32) + dot(place[...], ret[...], 0, 0)
    js[...] = dh.T.astype(BF)
    hf[:, cols(t)] = dh.astype(BF)

    own_cols = pl.ds(pl.multiple_of(s * TOK, TOK), TOK)
    for j in range(NX):
        mine = jnp.logical_and(z == t, x == j)

        @pl.when(jnp.logical_not(mine))
        def _():
            remote(
                js.at[pl.ds(64 * j, 64), :],
                dt.at[:, own_cols],
                j_send.at[j],
                j_recv.at[x],
                t * NX + j,
                z,
            ).start()

        @pl.when(mine)
        def _():
            dt[:, own_cols] = js[pl.ds(64 * j, 64), :]

    def h_piece(tp):
        return hf.at[:, cols(tp)]

    def j_piece(tp):
        return dt.at[:, cols(tp, 512)]

    hg = gather(h_piece, lambda i: h_send.at[i], lambda i: h_recv.at[i])
    jg = gather(j_piece, lambda i: k_send.at[i], lambda i: k_recv.at[i])
    hg[0]()
    hg[1]()
    for j in range(NX):

        @pl.when(jnp.logical_not(jnp.logical_and(z == t, x == j)))
        def _():
            arrived(
                dt.at[:, pl.ds(pl.multiple_of(t * 512 + j * TOK, TOK), TOK)], j_recv.at[j]
            )

    jg[0]()
    hg[2]()
    dz = dot(hf[...], out_proj[...], 1, 0)
    dconv = (dz * gate_b[...].astype(F32)).astype(BF)
    hsend[...] = dconv

    @pl.when(s < NSP - 1)
    def _():
        remote(
            hsend.at[pl.ds(TOK - 16, 16), :], halo.at[0], j_send.at[4], j_recv.at[4], s + 1, t
        ).start()

    @pl.when(s > 0)
    def _():
        remote(hsend.at[pl.ds(0, 16), :], halo.at[1], j_send.at[5], j_recv.at[5], s - 1, t).start()

    jg[1]()
    g_b[...] = (dz * conv_out[...].astype(F32)).astype(BF)

    @pl.when(s > 0)
    def _():
        arrived(halo.at[0], j_recv.at[4])

    @pl.when(s == 0)
    def _():
        halo[0] = jnp.zeros((16, CH), BF)

    @pl.when(s < NSP - 1)
    def _():
        arrived(halo.at[1], j_recv.at[5])

    @pl.when(s == NSP - 1)
    def _():
        halo[1] = jnp.zeros((16, CH), BF)

    d = dconv.astype(F32)
    at_row = lax.broadcasted_iota(jnp.int32, (TOK, CH), 0)
    before_first = halo[0].astype(F32)[15:16, :]
    after_last = halo[1].astype(F32)[0:1, :]
    earlier_rows = jnp.where(at_row == 0, before_first, pltpu.roll(d, 1, 0))
    later_rows = jnp.where(at_row == TOK - 1, after_last, pltpu.roll(d, TOK - 1, 0))
    tp3 = taps[...]
    grad_u = tp3[0:1, :] * later_rows + tp3[1:2, :] * d + tp3[2:3, :] * earlier_rows
    g_c[...] = (grad_u * value_v[...].astype(F32)).astype(BF)
    g_v[...] = (grad_u * gate_c[...].astype(F32)).astype(BF)

    for d in range(NZ):
        for i, source in enumerate((x_down, x_up, x_far)):
            arrived(block((z + d) % NZ, source), m_recv.at[3 * d + i])
    jg[2]()
    g_out[...] = dot(dt[...], mx[...], 1, 0)
    late = [
        pltpu.make_async_copy(a, b, o_sem.at[3 + i])
        for i, (a, b) in enumerate(((g_out, g_out_h), (g_b, g_b_h), (g_c, g_c_h), (g_v, g_v_h)))
    ]
    for store in late:
        store.start()
    stores += late

    for k in range(NK):
        each_x(1 if k == 0 else 0, lambda xx: a_copy(k, xx).wait_send())
        each_x(1 if k == 0 else 0, lambda xx: e_copy(k, xx).wait_send())
        chunk[k][4]()
    for m in range(NP):
        left(part.at[0, :, d_rows(m), :], d_send.at[m * 4])
        for i in range(3):
            left(along.at[i, d_rows(m), :], d_send.at[m * 4 + 1 + i])
    hg[3]()
    jg[3]()
    for d in range(NZ):
        for i in range(3):
            left(block(z, x), m_send.at[3 * d + i])
    for r in range(1, 5):
        half = 0 if r == 4 else None
        left(block(z, x, half), n_send.at[2 * r])
        left(block(z, x, half), n_send.at[2 * r + 1])
    for j in range(NX):

        @pl.when(jnp.logical_not(jnp.logical_and(z == t, x == j)))
        def _():
            left(js.at[pl.ds(64 * j, 64), :], j_send.at[j])

    @pl.when(s < NSP - 1)
    def _():
        left(halo.at[0], j_send.at[4])

    @pl.when(s > 0)
    def _():
        left(halo.at[1], j_send.at[5])

    for store in stores:
        store.wait()


def emit(*refs):
    ins, outs, held = refs[:7], refs[7:14], refs[14:21]
    i_sem, o_sem = refs[21:]
    pieces = []
    for a, b, v in zip(ins, outs, held):
        if len(a.shape) == 3:
            half = a.shape[1] // 2
            pieces += [tuple(r.at[:, pl.ds(i * half, half), :] for r in (a, b, v)) for i in range(2)]
        else:
            pieces.append((a, b, v))
    loads = [pltpu.make_async_copy(a, v, i_sem.at[i]) for i, (a, _, v) in enumerate(pieces)]
    stores = [pltpu.make_async_copy(v, b, o_sem.at[i]) for i, (_, b, v) in enumerate(pieces)]
    for load in loads:
        load.start()
    for load, store in zip(loads, stores):
        load.wait()
        store.start()
    for store in stores:
        store.wait()


def local(
    out_grad,
    moe_input,
    route_weight,
    route_ids,
    gate_proj,
    up_proj,
    down_proj,
    out_proj,
    conv_out,
    gate_b,
    gate_c,
    value_v,
    conv_taps,
):
    hbm = pl.BlockSpec(memory_space=pl.ANY)
    dma = pltpu.SemaphoreType.DMA
    shape = jax.ShapeDtypeStruct
    kept = pl.pallas_call(
        kernel,
        out_shape=(
            shape((1, FFL, D), BF),
            shape((1, FFL, D), BF),
            shape((1, FFL, D), BF),
            shape((64, CH), F32),
            shape((TOK, CH), BF),
            shape((TOK, CH), BF),
            shape((TOK, CH), BF),
        ),
        in_specs=[hbm] * 13,
        out_specs=(hbm,) * 7,
        scratch_shapes=[
            pltpu.VMEM((TOK, CH), BF),
            pltpu.VMEM((TOK, CH), BF),
            pltpu.VMEM((2, TOK), F32),
            pltpu.VMEM((2, TOK), jnp.int32),
            pltpu.VMEM((D, CH), BF),
            pltpu.VMEM((TOK, CH), BF),
            pltpu.VMEM((TOK, CH), BF),
            pltpu.VMEM((TOK, CH), BF),
            pltpu.VMEM((TOK, CH), BF),
            pltpu.VMEM((3, CH), F32),
            pltpu.VMEM((64, CH), F32),
            pltpu.VMEM((TOK, CH), BF),
            pltpu.VMEM((TOK, CH), BF),
            pltpu.VMEM((TOK, CH), BF),
            pltpu.VMEM((2 * FFL, D), BF),
            pltpu.VMEM((FFL, D), BF),
            dma((10,)),
            dma((7,)),
            pltpu.VMEM((2, ROWS, CH), BF),
            pltpu.VMEM((2, ROWS, D), BF),
            pltpu.VMEM((2 * FFL, D), BF),
            pltpu.VMEM((FFL, D), BF),
            pltpu.VMEM((ROWS, TOK), BF),
            pltpu.VMEM((2 * FFL, ROWS), BF),
            pltpu.VMEM((FFL, ROWS), BF),
            pltpu.VMEM((2, NY, ROWS, CH), BF),
            pltpu.VMEM((NY, ROWS, CH), BF),
            pltpu.VMEM((NY, ROWS, CH), BF),
            pltpu.VMEM((3, ROWS, CH), BF),
            pltpu.VMEM((ROWS, CH), BF),
            pltpu.VMEM((ROWS, CH), BF),
            pltpu.VMEM((TOK, D), BF),
            pltpu.VMEM((CH, TOK), BF),
            pltpu.VMEM((64, NSP * TOK), BF),
            pltpu.VMEM((NSP * TOK, CH), BF),
            pltpu.VMEM((TOK, CH), BF),
            pltpu.VMEM((2, 16, CH), BF),
            dma((3,)),
            dma((NSP,)),
            dma((NSP,)),
            dma((9 * NK,)),
            dma((9 * NK,)),
            dma((4 * NP,)),
            dma((4 * NP,)),
            dma((NSP,)),
            dma((NSP,)),
            dma((7,)),
            dma((7,)),
            dma((6,)),
            dma((6,)),
            dma((7,)),
            dma((7,)),
            dma((3 * NZ,)),
            dma((3 * NZ,)),
            dma((10,)),
            dma((10,)),
        ],
        compiler_params=pltpu.CompilerParams(
            collective_id=0, has_side_effects=True, vmem_limit_bytes=60 * 1024 * 1024
        ),
        name="layer",
    )(
        out_grad,
        moe_input,
        route_weight.T,
        route_ids.T,
        gate_proj.transpose(0, 2, 1),
        up_proj.transpose(0, 2, 1),
        down_proj,
        out_proj,
        conv_out,
        gate_b,
        gate_c,
        value_v,
        conv_taps,
    )
    g_gate, g_up, g_down, g_out, g_b, g_c, g_v = pl.pallas_call(
        emit,
        out_shape=tuple(shape(a.shape, a.dtype) for a in kept),
        in_specs=[hbm] * 7,
        out_specs=(hbm,) * 7,
        scratch_shapes=[pltpu.VMEM(a.shape, a.dtype) for a in kept] + [dma((10,)), dma((10,))],
        compiler_params=pltpu.CompilerParams(vmem_limit_bytes=60 * 1024 * 1024),
        name="emit",
    )(*kept)
    return g_gate.transpose(0, 2, 1), g_up.transpose(0, 2, 1), g_down, g_out, g_b, g_c, g_v


def solution(mesh):
    return jax.shard_map(
        local,
        mesh=mesh,
        in_specs=(
            P("sp", "tp"),
            P("sp", "tp"),
            P("sp", None),
            P("sp", None),
            P("sp", None, "tp"),
            P("sp", None, "tp"),
            P("sp", "tp", None),
            P(None, "tp"),
            P("sp", "tp"),
            P("sp", "tp"),
            P("sp", "tp"),
            P("sp", "tp"),
            P(None, "tp"),
        ),
        out_specs=(
            P("sp", None, "tp"),
            P("sp", None, "tp"),
            P("sp", "tp", None),
            P("sp", "tp"),
            P("sp", "tp"),
            P("sp", "tp"),
            P("sp", "tp"),
        ),
        check_vma=False,
    )
```

time: 109 us -> 92.8 us (0.85)
  local copies, waits for them, and re-layouts: 13.5 us -> 0 us
  Pallas kernels: 94.3 us -> 92.1 us
    unnamed x22 -> x0, local copies, waits for them, and re-layouts: 9.31 us -> none
    pallas_call x2 -> x0, local copies, waits for them, and re-layouts: 4.24 us -> none  [local(): pl.pallas_call(kernel, out_shape=(shape((1, D, FFL), BF), shape((1, D, FF...]
    pallas_call x1 -> x2, Pallas kernels: 94.3 us -> 92.1 us  [the longest x1 88.4 us: local(): pl.pallas_call(kernel, out_shape=(shape((1, FFL, D), BF), shape((1, FFL,...]
where the time goes in v2:
time: 92.8 us; the launch traced here: 92.7 us
  Pallas kernels  92.1 us (99%)
    pallas_call x1, Pallas kernels, local(): pl.pallas_call(kernel, out_shape=(shape((1, FFL, D), BF), shape((1, FFL,...  88.4 us
    pallas_call x1, Pallas kernels, local(): pl.pallas_call(emit, out_shape=tuple((shape(a.shape, a.dtype) for a in ke...  3.72 us

profile of v2, /device:TPU:1, one launch (start us, length us, event | category | flops | bytes accessed | tf_op | source)
XLA Modules:
  0.0 92.7 jit_solution(3260530682159146848)
XLA Ops:
  0.6 88.4 %layer.1 = (bf16[1,352,2048]{2,1,0:T(8,128)(2,1)}, bf16[1,352,2048]{2,1,0:T(8,128)(2,1)}, bf16[1,352,2048]{2,1,0:T(8,128)(2,1)}, f32[64,256]{1,0:T(8,128)}, bf16...) custom-call(bf16[128,256]{1,0:T(8,128)(2,1)} %out_grad_h.1, ...), custom_call_target="tpu_custom_call" | custom-call | tf_op jit(solution)/shard_map/layer/pallas_call | solution.py:672
  89.0 3.7 %emit.1 = (bf16[1,352,2048]{2,1,0:T(8,128)(2,1)}, bf16[1,352,2048]{2,1,0:T(8,128)(2,1)}, bf16[1,352,2048]{2,1,0:T(8,128)(2,1)}, f32[64,256]{1,0:T(8,128)}, bf16[...) custom-call(bf16[1,352,2048]{2,1,0:T(8,128)(2,1)} %get-tuple-element.21.refs_0_, ...), custom_call_target="tpu_custom_call" | custom-call | tf_op jit(solution)/shard_map/emit/pallas_call | solution.py:762

commit v3 on v2

--- a/solution.py
+++ b/solution.py
@@ -20,7 +20,7 @@
 CR = ROWS // NK
 NP = 4
 PR = ROWS // NP
-ORDER = (0, 1, 7, 4, 3, 5, 2, 6)
+ORDER = (0, 1, 7, 3, 5, 4, 2, 6)
 
 
 def dot(a, b, ca, cb):
@@ -140,13 +140,15 @@
     lax.fori_loop(1, NSP, greet, 0)
     for peer in (t_up, t_down, t_far, t_sib):
         pl.semaphore_signal(barrier, inc=1, device_id={"sp": s, "tp": peer}, device_id_type=MESH)
+    cross = (z + NZ // 2) % NZ
+    back = (t + NZ // 2) % NZ
     for j in range(NX):
-
-        @pl.when(jnp.logical_not(jnp.logical_and(z == t, x == j)))
-        def _():
-            pl.semaphore_signal(
-                barrier, inc=1, device_id={"sp": t * NX + j, "tp": z}, device_id_type=MESH
-            )
+        pl.semaphore_signal(
+            barrier, inc=1, device_id={"sp": t * NX + j, "tp": cross}, device_id_type=MESH
+        )
+        pl.semaphore_signal(
+            barrier, inc=1, device_id={"sp": back * NX + j, "tp": z}, device_id_type=MESH
+        )
 
     small = [
         pltpu.make_async_copy(a, b, i_sem.at[i])
@@ -202,13 +204,13 @@
     send[0] = dot(p0 + p1, moe_input[...], 1, 0).astype(BF)
     send[1] = (dot(p0, dy0, 1, 0) + dot(p1, dy1, 1, 0)).astype(BF)
     mixed = (gate_b[...].astype(F32) * conv_out[...].astype(F32)).astype(BF)
-    own_rows = pl.ds(pl.multiple_of(s * TOK, TOK), TOK)
+    own_rows = pl.ds(pl.multiple_of((x * NZ + z) * TOK, TOK), TOK)
     mx[own_rows, :] = mixed
 
     def cols(tp, width=CH):
         return pl.ds(pl.multiple_of(tp * width, width), width)
 
-    pl.semaphore_wait(barrier, NSP - 1 + 4 + 4 - jnp.where(z == t, 1, 0))
+    pl.semaphore_wait(barrier, NSP - 1 + 4 + 8)
 
     def a_copy(k, xx):
         target = ((z + ORDER[k]) % NZ) * NX + xx
@@ -308,7 +310,7 @@
     ]
 
     def block(zz, xx, half=None):
-        base = (zz * NX + xx) * TOK
+        base = (xx * NZ + zz) * TOK
         if half is None:
             return mx.at[pl.ds(pl.multiple_of(base, TOK), TOK), :]
         return mx.at[pl.ds(pl.multiple_of(base + half * (TOK // 2), TOK // 2), TOK // 2), :]
@@ -425,57 +427,62 @@
     for k in range(NK):
         a_wait(k)
         chunk[k][0]()
-        if k >= 1:
-            chunk[k - 1][1]()
         if k >= 2:
-            chunk[k - 2][2]()
-        if k == 3:
+            chunk[k - 2][1]()
+        if k >= 4:
+            chunk[k - 4][2]()
+        if k == 4:
             z_arrived(1)
             z_hop(2)
             x_hop(1)
             x_hop(7)
-        if k == 5:
+        if k == 6:
             z_arrived(2)
             z_hop(3)
             x_hop(2)
             x_hop(6)
-    for k in range(4):
-        chunk[k][3]()
+    chunk[6][1]()
+    chunk[4][2]()
     for load in loads:
         load.wait()
+    chunk[0][3]()
+    chunk[1][3]()
+    chunk[2][3]()
+    chunk[3][3]()
     forward(0, 4)
     chunk[7][1]()
-    chunk[6][2]()
+    chunk[5][2]()
     dx(0)
     d0(0)
-    chunk[7][2]()
+    chunk[6][2]()
+    dx(1)
+    d0(1)
+    d1(0)
     z_arrived(3)
     z_hop(4)
     x_hop(3)
     x_hop(5)
-    dx(1)
-    d0(1)
-    d1(0)
+    chunk[7][2]()
     chunk[4][3]()
     chunk[5][3]()
     forward(4, 6)
     d1(1)
     dx(2)
     d0(2)
-    d3(0)
     chunk[6][3]()
     chunk[7][3]()
     forward(6, 8)
     d1(2)
     dx(3)
     d0(3)
+    d3(0)
     z_arrived(4)
     x_hop(4)
     d3(1)
-    grads(0, 1)
     d1(3)
+    grads(0, 2)
     d3(2)
-    grads(1, 4)
+    grads(2, 4)
     d3(3)
     grads(4, 8)
     stores = [
@@ -499,44 +506,41 @@
     js[...] = dh.T.astype(BF)
     hf[:, cols(t)] = dh.astype(BF)
 
-    own_cols = pl.ds(pl.multiple_of(s * TOK, TOK), TOK)
+    def token_cols(zz, xx):
+        return pl.ds(pl.multiple_of((xx * NZ + zz) * TOK, TOK), TOK)
+
     for j in range(NX):
-        mine = jnp.logical_and(z == t, x == j)
-
-        @pl.when(jnp.logical_not(mine))
-        def _():
-            remote(
-                js.at[pl.ds(64 * j, 64), :],
-                dt.at[:, own_cols],
-                j_send.at[j],
-                j_recv.at[x],
-                t * NX + j,
-                z,
-            ).start()
-
-        @pl.when(mine)
-        def _():
-            dt[:, own_cols] = js[pl.ds(64 * j, 64), :]
+        remote(
+            js.at[pl.ds(64 * j, 64), :],
+            dt.at[:, token_cols(z, x)],
+            j_send.at[j],
+            j_recv.at[x],
+            t * NX + j,
+            cross,
+        ).start()
 
     def h_piece(tp):
         return hf.at[:, cols(tp)]
 
-    def j_piece(tp):
-        return dt.at[:, cols(tp, 512)]
+    x_order = (x, (x + 1) % NX, (x + NX - 1) % NX, (x + 2) % NX)
+
+    def j_piece(i):
+        return lambda tp: dt.at[:, token_cols((tp + NZ // 2) % NZ, x_order[i])]
 
     hg = gather(h_piece, lambda i: h_send.at[i], lambda i: h_recv.at[i])
-    jg = gather(j_piece, lambda i: k_send.at[i], lambda i: k_recv.at[i])
+    jg = [
+        gather(
+            j_piece(i),
+            lambda n, i=i: k_send.at[7 * i + n],
+            lambda n, i=i: k_recv.at[7 * i + n],
+        )
+        for i in range(NX)
+    ]
     hg[0]()
     hg[1]()
-    for j in range(NX):
-
-        @pl.when(jnp.logical_not(jnp.logical_and(z == t, x == j)))
-        def _():
-            arrived(
-                dt.at[:, pl.ds(pl.multiple_of(t * 512 + j * TOK, TOK), TOK)], j_recv.at[j]
-            )
-
-    jg[0]()
+    for i in range(NX):
+        arrived(dt.at[:, token_cols(back, x_order[i])], j_recv.at[x_order[i]])
+        jg[i][0]()
     hg[2]()
     dz = dot(hf[...], out_proj[...], 1, 0)
     dconv = (dz * gate_b[...].astype(F32)).astype(BF)
@@ -552,7 +556,8 @@
     def _():
         remote(hsend.at[pl.ds(0, 16), :], halo.at[1], j_send.at[5], j_recv.at[5], s - 1, t).start()
 
-    jg[1]()
+    for i in range(NX):
+        jg[i][1]()
     g_b[...] = (dz * conv_out[...].astype(F32)).astype(BF)
 
     @pl.when(s > 0)
@@ -585,8 +590,12 @@
     for d in range(NZ):
         for i, source in enumerate((x_down, x_up, x_far)):
             arrived(block((z + d) % NZ, source), m_recv.at[3 * d + i])
-    jg[2]()
-    g_out[...] = dot(dt[...], mx[...], 1, 0)
+    total = jnp.zeros((64, CH), F32)
+    for i in range(NX):
+        jg[i][2]()
+        ks = pl.ds(pl.multiple_of(x_order[i] * (NZ * TOK), NZ * TOK), NZ * TOK)
+        total += dot(dt[:, ks], mx[ks, :], 1, 0)
+    g_out[...] = total
     late = [
         pltpu.make_async_copy(a, b, o_sem.at[3 + i])
         for i, (a, b) in enumerate(((g_out, g_out_h), (g_b, g_b_h), (g_c, g_c_h), (g_v, g_v_h)))
@@ -604,7 +613,8 @@
         for i in range(3):
             left(along.at[i, d_rows(m), :], d_send.at[m * 4 + 1 + i])
     hg[3]()
-    jg[3]()
+    for i in range(NX):
+        jg[i][3]()
     for d in range(NZ):
         for i in range(3):
             left(block(z, x), m_send.at[3 * d + i])
@@ -613,10 +623,7 @@
         left(block(z, x, half), n_send.at[2 * r])
         left(block(z, x, half), n_send.at[2 * r + 1])
     for j in range(NX):
-
-        @pl.when(jnp.logical_not(jnp.logical_and(z == t, x == j)))
-        def _():
-            left(js.at[pl.ds(64 * j, 64), :], j_send.at[j])
+        left(js.at[pl.ds(64 * j, 64), :], j_send.at[j])
 
     @pl.when(s < NSP - 1)
     def _():
@@ -733,8 +740,8 @@
             dma((7,)),
             dma((6,)),
             dma((6,)),
-            dma((7,)),
-            dma((7,)),
+            dma((7 * NX,)),
+            dma((7 * NX,)),
             dma((3 * NZ,)),
             dma((3 * NZ,)),
             dma((10,)),

time: 92.8 us -> 83.5 us (0.90)
  Pallas kernels: 92.1 us -> 82.1 us
    pallas_call x1, Pallas kernels: 88.4 us -> 78.3 us  [local(): pl.pallas_call(kernel, out_shape=(shape((1, FFL, D), BF), shape((1, FFL,...]
where the time goes in v3:
time: 83.5 us; the launch traced here: 82.7 us
  Pallas kernels  82.1 us (98%)
    pallas_call x1, Pallas kernels, local(): pl.pallas_call(kernel, out_shape=(shape((1, FFL, D), BF), shape((1, FFL,...  78.3 us
    pallas_call x1, Pallas kernels, local(): pl.pallas_call(emit, out_shape=tuple((shape(a.shape, a.dtype) for a in ke...  3.72 us

profile of v3, /device:TPU:1, one launch (start us, length us, event | category | flops | bytes accessed | tf_op | source)
XLA Modules:
  0.0 82.7 jit_solution(2137511217505811296)
XLA Ops:
  0.6 78.3 %layer.1 = (bf16[1,352,2048]{2,1,0:T(8,128)(2,1)}, bf16[1,352,2048]{2,1,0:T(8,128)(2,1)}, bf16[1,352,2048]{2,1,0:T(8,128)(2,1)}, f32[64,256]{1,0:T(8,128)}, bf16...) custom-call(bf16[128,256]{1,0:T(8,128)(2,1)} %out_grad_h.1, ...), custom_call_target="tpu_custom_call" | custom-call | tf_op jit(solution)/shard_map/layer/pallas_call | solution.py:679
  79.0 3.7 %emit.1 = (bf16[1,352,2048]{2,1,0:T(8,128)(2,1)}, bf16[1,352,2048]{2,1,0:T(8,128)(2,1)}, bf16[1,352,2048]{2,1,0:T(8,128)(2,1)}, f32[64,256]{1,0:T(8,128)}, bf16[...) custom-call(bf16[1,352,2048]{2,1,0:T(8,128)(2,1)} %get-tuple-element.21.refs_0_, ...), custom_call_target="tpu_custom_call" | custom-call | tf_op jit(solution)/shard_map/emit/pallas_call | solution.py:769

commit v4 on v3

--- a/solution.py
+++ b/solution.py
@@ -482,9 +482,8 @@
     d1(3)
     grads(0, 2)
     d3(2)
-    grads(2, 4)
     d3(3)
-    grads(4, 8)
+    grads(2, 8)
     stores = [
         pltpu.make_async_copy(og_gu.at[pl.ds(0, FFL), :], g_gate.at[0], o_sem.at[0]),
         pltpu.make_async_copy(og_gu.at[pl.ds(FFL, FFL), :], g_up.at[0], o_sem.at[1]),
@@ -537,6 +536,21 @@
         for i in range(NX)
     ]
     hg[0]()
+    for k in range(NK):
+        each_x(1 if k == 0 else 0, lambda xx: a_copy(k, xx).wait_send())
+        each_x(1 if k == 0 else 0, lambda xx: e_copy(k, xx).wait_send())
+        chunk[k][4]()
+    for m in range(NP):
+        left(part.at[0, :, d_rows(m), :], d_send.at[m * 4])
+        for i in range(3):
+            left(along.at[i, d_rows(m), :], d_send.at[m * 4 + 1 + i])
+    for d in range(NZ):
+        for i in range(3):
+            left(block(z, x), m_send.at[3 * d + i])
+    for r in range(1, 5):
+        half = 0 if r == 4 else None
+        left(block(z, x, half), n_send.at[2 * r])
+        left(block(z, x, half), n_send.at[2 * r + 1])
     hg[1]()
     for i in range(NX):
         arrived(dt.at[:, token_cols(back, x_order[i])], j_recv.at[x_order[i]])
@@ -604,24 +618,9 @@
         store.start()
     stores += late
 
-    for k in range(NK):
-        each_x(1 if k == 0 else 0, lambda xx: a_copy(k, xx).wait_send())
-        each_x(1 if k == 0 else 0, lambda xx: e_copy(k, xx).wait_send())
-        chunk[k][4]()
-    for m in range(NP):
-        left(part.at[0, :, d_rows(m), :], d_send.at[m * 4])
-        for i in range(3):
-            left(along.at[i, d_rows(m), :], d_send.at[m * 4 + 1 + i])
     hg[3]()
     for i in range(NX):
         jg[i][3]()
-    for d in range(NZ):
-        for i in range(3):
-            left(block(z, x), m_send.at[3 * d + i])
-    for r in range(1, 5):
-        half = 0 if r == 4 else None
-        left(block(z, x, half), n_send.at[2 * r])
-        left(block(z, x, half), n_send.at[2 * r + 1])
     for j in range(NX):
         left(js.at[pl.ds(64 * j, 64), :], j_send.at[j])
 

time: 83.5 us -> 83.1 us (level)
  no operation moved by 1% of the time
where the time goes in v4:
time: 83.1 us; the launch traced here: 82.3 us
  Pallas kernels  81.6 us (98%)
    pallas_call x1, Pallas kernels, local(): pl.pallas_call(kernel, out_shape=(shape((1, FFL, D), BF), shape((1, FFL,...  77.9 us
    pallas_call x1, Pallas kernels, local(): pl.pallas_call(emit, out_shape=tuple((shape(a.shape, a.dtype) for a in ke...  3.72 us

profile of v4, /device:TPU:1, one launch (start us, length us, event | category | flops | bytes accessed | tf_op | source)
XLA Modules:
  0.0 82.3 jit_solution(9718881380525151221)
XLA Ops:
  0.6 77.9 %layer.1 = (bf16[1,352,2048]{2,1,0:T(8,128)(2,1)}, bf16[1,352,2048]{2,1,0:T(8,128)(2,1)}, bf16[1,352,2048]{2,1,0:T(8,128)(2,1)}, f32[64,256]{1,0:T(8,128)}, bf16...) custom-call(bf16[128,256]{1,0:T(8,128)(2,1)} %out_grad_h.1, ...), custom_call_target="tpu_custom_call" | custom-call | tf_op jit(solution)/shard_map/layer/pallas_call | solution.py:678
  78.6 3.7 %emit.1 = (bf16[1,352,2048]{2,1,0:T(8,128)(2,1)}, bf16[1,352,2048]{2,1,0:T(8,128)(2,1)}, bf16[1,352,2048]{2,1,0:T(8,128)(2,1)}, f32[64,256]{1,0:T(8,128)}, bf16[...) custom-call(bf16[1,352,2048]{2,1,0:T(8,128)(2,1)} %get-tuple-element.21.refs_0_, ...), custom_call_target="tpu_custom_call" | custom-call | tf_op jit(solution)/shard_map/emit/pallas_call | solution.py:768
